TPU v7x, 256 devices: a whole 4x4x8 slice. The times are simulated.
256 devices in a mesh: ra: 32 (over z, y), cb: 4 (over x), dp: 2 (over core).
Axes of the slice: x: 4, y: 4, z: 8, core: 2. Of those that a mesh axis runs over, the one named last changes fastest.
Arguments:
- stream: bfloat16 [4, 64, 4096], P('dp', None, 'ra'), may hold values from -16 to 16
- norm_gain: bfloat16 [2, 4096], P(None, 'ra'), may hold values from 0.099609375 to 1.8984375
- gate_weight: bfloat16 [2, 4096, 12288], P(None, 'ra', 'cb'), may hold values from -0.09375 to 0.09375
- value_weight: bfloat16 [2, 4096, 12288], P(None, 'ra', 'cb'), may hold values from -0.09375 to 0.09375
- gate_taps: bfloat16 [2, 3, 12288], P(None, None, 'cb'), may hold values from -3 to 3
- value_taps: bfloat16 [2, 3, 12288], P(None, None, 'cb'), may hold values from -3 to 3
- gate_bias: bfloat16 [2, 12288], P(None, 'cb'), may hold values from -3 to 3
- value_bias: bfloat16 [2, 12288], P(None, 'cb'), may hold values from -3 to 3
- down_weight: bfloat16 [2, 12288, 4096], P(None, 'cb', 'ra'), may hold values from -0.0546875 to 0.0546875
- final_gain: bfloat16 [4096], P('ra'), may hold values from 0.099609375 to 1.8984375
Outputs:
- mixed: bfloat16 [4, 64, 4096], P('dp', None, 'ra')
All inputs are finite; a program needn't handle non-finite values.
Results may differ from a plain program's by a relative error of at most 0.035.
Values may be sent and summed in bfloat16 or wider, within the bound.
No kernel may reach another device: no remote copies, remote signals or barrier semaphores. Data moves between devices by JAX's collectives and lax.ppermute only.
A program may use at most 64 MiB of HBM per device.

v0:
```python
import functools

import jax
import jax.numpy as jnp
from jax import lax
from jax.experimental import pallas as pl
from jax.experimental.pallas import tpu as pltpu
from jax.sharding import Mesh
from jax.sharding import PartitionSpec as P


D = 4096
LAYERS = 2
LANES = 128
EXTRA = 8
WHOLE_VMEM = 67043328
EPS = 1e-06
F32 = jnp.float32
BF16 = jnp.bfloat16
VMEM = pl.BlockSpec(memory_space=pltpu.VMEM)
HBM = pl.BlockSpec(memory_space=pltpu.MemorySpace.HBM)


def exchanged(x, axis):
    return lax.all_to_all(x, axis, split_axis=0, concat_axis=0, tiled=True)


def room(mebibytes):
    return pltpu.CompilerParams(vmem_limit_bytes=mebibytes * 1024 * 1024)


def cost(flops, moved):
    return pl.CostEstimate(flops=flops, bytes_accessed=moved, transcendentals=0)


def up_copies(up, layer, ny, at, out, start, sems, first):
    width, columns = up.shape[1:]
    each = columns // ny // LANES
    for j in range(each):
        low = pl.multiple_of((at * each + j) * LANES, LANES)
        yield pltpu.make_async_copy(
            up.at[layer, :, pl.ds(low, LANES)],
            out.at[pl.ds(start + j * width, width), :],
            sems.at[first + j],
        )


def down_copies(down, ny, core, at, out, start, sems, first):
    half = down.shape[1] // ny // 2
    low = pl.multiple_of((at * 2 + core) * half, half)
    for layer in range(LAYERS):
        yield pltpu.make_async_copy(
            down.at[layer, pl.ds(low, half), :],
            out.at[pl.ds(start + layer * half, half), :],
            sems.at[first + layer],
        )


def pack_first_kernel(ny, gate, value, stream, gain, out, held, sems, more):
    tokens, width = stream.shape
    each = gate.shape[2] // ny // LANES
    start = tokens + LAYERS * 8
    core = lax.axis_index("dp")
    others = [
        pltpu.make_async_copy(stream, out.at[i, pl.ds(0, tokens), :], more.at[i]) for i in range(ny)
    ]
    others.append(pltpu.make_async_copy(gain, held, more.at[ny]))

    def copies(up):
        for i in range(ny):
            yield from up_copies(up, 0, ny, i, out.at[i], start, sems, i * each)

    @pl.when(core == 0)
    def _():
        for c in copies(gate):
            c.start()

    @pl.when(core == 1)
    def _():
        for c in copies(value):
            c.start()

    for c in others:
        c.start()
    others[-1].wait()
    gains = jnp.broadcast_to(held[...].astype(F32)[:, None, :], (LAYERS, 8, width))
    gains = gains.reshape(LAYERS * 8, width).astype(BF16)
    for i in range(ny):
        out[i, tokens : tokens + LAYERS * 8, :] = gains
    for c in others[:-1]:
        c.wait()
    for c in copies(gate):
        c.wait()


def packed_first(ny, gate, value, stream, gain):
    rows = gate.shape[1] * gate.shape[2] // ny // LANES
    rows += stream.shape[0] + LAYERS * 8
    each = gate.shape[2] // ny // LANES
    return pl.pallas_call(
        functools.partial(pack_first_kernel, ny),
        out_shape=jax.ShapeDtypeStruct((ny, rows, LANES), BF16),
        in_specs=[HBM] * 4,
        out_specs=VMEM,
        scratch_shapes=[
            pltpu.VMEM(gain.shape, BF16),
            pltpu.SemaphoreType.DMA((ny * each,)),
            pltpu.SemaphoreType.DMA((ny + 1,)),
        ],
        cost_estimate=cost(1000000, 2 * ny * rows * LANES),
        compiler_params=pltpu.CompilerParams(
            vmem_limit_bytes=WHOLE_VMEM - 2 * ny * rows * LANES - 16384
        ),
        name="pack0",
    )(gate, value, stream, gain)


def pack_second_kernel(ny, gate, value, down, *refs):
    outs, sems = refs[:-1], refs[-1]
    ups = gate.shape[2] // ny // LANES
    each = ups + LAYERS
    core = lax.axis_index("dp")
    y = lax.axis_index("y")

    def copies(up, spare):
        for k in range(ny + 1):
            at = lax.rem(y + k, ny) if k < ny else y
            side = core if k < ny else 1 - core
            first = k * each
            yield from up_copies(up if k < ny else spare, 1, ny, at, outs[k], 0, sems, first)
            low = outs[ny + 1 + k]
            yield from down_copies(down, ny, side, at, low, 0, sems, first + ups)

    @pl.when(core == 0)
    def _():
        for c in copies(gate, value):
            c.start()

    @pl.when(core == 1)
    def _():
        for c in copies(value, gate):
            c.start()

    for c in copies(gate, value):
        c.wait()


def packed_second(ny, gate, value, down):
    rows = gate.shape[1] * gate.shape[2] // ny // LANES
    low = LAYERS * down.shape[1] // ny // 2
    each = gate.shape[2] // ny // LANES + LAYERS
    return pl.pallas_call(
        functools.partial(pack_second_kernel, ny),
        out_shape=[jax.ShapeDtypeStruct((rows, LANES), BF16)] * (ny + 1)
        + [jax.ShapeDtypeStruct((low, LANES), BF16)] * (ny + 1),
        in_specs=[HBM] * 3,
        out_specs=[VMEM] * (2 * ny + 2),
        scratch_shapes=[pltpu.SemaphoreType.DMA(((ny + 1) * each,))],
        cost_estimate=cost(1000000, 2 * ny * rows * LANES),
        compiler_params=room(4),
        name="pack1",
    )(gate, value, down)


def high_and_low(squares):
    tokens = squares.shape[0]
    total = jnp.broadcast_to(jnp.sum(squares, axis=1, keepdims=True), (tokens, LANES)).T[0:EXTRA]
    high = total.astype(BF16).astype(F32)
    index = lax.broadcasted_iota(jnp.int32, (EXTRA, tokens), 0)
    return jnp.where(index == 0, high, jnp.where(index == 1, total - high, 0.0)).astype(BF16)


def multiplied(gained, weights, start, block, store):
    width = LANES
    wide = 2 * LANES
    for j in range(block // wide):
        weight = jnp.concatenate(
            [
                jnp.concatenate(
                    [w[pl.ds(start + (2 * j + i) * width, width), :] for i in range(2)], axis=1
                )
                for w in weights
            ],
            axis=0,
        )
        store(j * wide, jnp.dot(gained, weight, preferred_element_type=F32).T.astype(BF16))


def into_slots(out, rows, units):
    def store(first, result):
        low, end = first, first + result.shape[0]
        while low < end:
            slot = low // units
            high = min(end, (slot + 1) * units)
            out[slot, pl.ds(rows + (low - slot * units), high - low), :] = result[
                low - first : high - first
            ]
            low = high

    return store


def with_gain(values, gain_block, layer):
    return (values * gain_block.astype(F32)[8 * layer : 8 * layer + 1]).astype(BF16)


def first_up_kernel(side, start, ny, nz, block, *refs):
    mine = refs[0]
    out = refs[1] if side == 0 else refs[3]
    tokens = LANES
    units = block // nz
    core = lax.axis_index("dp")
    gained = jnp.concatenate(
        [
            with_gain(mine[k, 0:tokens, :].astype(F32), mine[k, tokens : tokens + 16, :], 0)
            for k in range(ny)
        ],
        axis=1,
    )
    if side == 0:
        weights = [mine.at[k] for k in range(ny)]
        multiplied(gained, weights, start, block, into_slots(out, 0, units))
        return
    other, near = refs[1], refs[2]
    weights = [other.at[k] for k in range(ny)]
    rows = pl.multiple_of((1 - core) * units, 16)
    multiplied(gained, weights, start, block, into_slots(out, rows, units))
    squares = jnp.zeros((tokens, LANES), F32)
    for k in range(ny):
        values = mine[k, 0:tokens, :].astype(F32)
        squares = squares + values * values
    both = high_and_low(squares)
    rows = pl.multiple_of(core * units, 16)
    refs[4][...] = mine[:, 0:start, :]
    for i in range(nz):
        out[i, pl.ds(rows, units), :] = near[i]
        out[i, 2 * units : 2 * units + EXTRA, :] = both


def first_projected(side, start, block, ny, nz, args):
    units = block // nz
    rows = units if side == 0 else 2 * units + EXTRA
    shapes = [jax.ShapeDtypeStruct((nz, rows, LANES), BF16)]
    if side:
        shapes.append(jax.ShapeDtypeStruct((ny, start, LANES), BF16))
    return pl.pallas_call(
        functools.partial(first_up_kernel, side, start, ny, nz, block),
        out_shape=shapes,
        in_specs=[VMEM] * len(args),
        out_specs=[VMEM] * len(shapes),
        cost_estimate=cost(2 * ny * LANES * LANES * block, 2 * ny * LANES * block),
        compiler_params=room(8),
    )(*args)


def second_up_kernel(ny, nz, block, *refs):
    mine, fresh = refs[:2]
    sides = [refs[2 : 2 + ny], refs[2 + ny : 2 + 2 * ny]]
    out, kept = refs[2 + 2 * ny :]
    tokens = LANES
    units = block // nz
    core = lax.axis_index("dp")
    y = lax.axis_index("y")
    squares = jnp.zeros((tokens, LANES), F32)
    gained = []
    for k in range(ny):
        at = lax.rem(y - k + ny, ny)
        values = fresh[:, at].astype(F32).reshape(tokens, LANES)
        if k == 0:
            kept[...] = values.astype(BF16)
        squares = squares + values * values
        gained.append(with_gain(values, mine[at, tokens : tokens + 16, :], 1))
    gained = jnp.concatenate(gained, axis=1)
    for side, weights in enumerate(sides):
        rows = pl.multiple_of((core if side == 0 else 1 - core) * units, 16)
        multiplied(gained, weights, 0, block, into_slots(out, rows, units))
    both = high_and_low(squares)
    for i in range(nz):
        out[i, 2 * units : 2 * units + EXTRA, :] = both


def second_projected(block, ny, nz, args):
    units = block // nz
    return pl.pallas_call(
        functools.partial(second_up_kernel, ny, nz, block),
        out_shape=[
            jax.ShapeDtypeStruct((nz, 2 * units + EXTRA, LANES), BF16),
            jax.ShapeDtypeStruct((LANES, LANES), BF16),
        ],
        in_specs=[VMEM] * len(args),
        out_specs=[VMEM] * 2,
        cost_estimate=cost(4 * ny * LANES * LANES * block, 4 * ny * LANES * block),
        compiler_params=room(8),
        name="up1",
    )(*args)


def mid_kernel(layer, length, parts, table, out):
    count, _, tokens = parts.shape
    units = out.shape[1]
    total = parts[0].astype(F32)
    for i in range(1, count):
        total = total + parts[i].astype(F32)
    mean = (total[2 * units : 2 * units + 1] + total[2 * units + 1 : 2 * units + 2]) / D
    scale = lax.rsqrt(mean + EPS)
    position = lax.rem(lax.broadcasted_iota(jnp.int32, (units, tokens), 1), length)
    spread = jnp.concatenate([table[layer]] * (LANES // 8), axis=0)
    columns = spread.T[0:units]

    def mixed(low, at):
        x = (total[low : low + units] * scale).astype(BF16).astype(F32)
        one = jnp.where(position >= 1, pltpu.roll(x, 1, 1), 0.0)
        two = jnp.where(position >= 2, pltpu.roll(x, 2, 1), 0.0)
        return (
            columns[:, at + 3 : at + 4]
            + two * columns[:, at : at + 1]
            + one * columns[:, at + 1 : at + 2]
            + x * columns[:, at + 2 : at + 3]
        )

    hidden = (jax.nn.gelu(mixed(0, 0)) * mixed(units, 4)).astype(BF16)
    for i in range(out.shape[0]):
        out[i] = hidden


def gated(layer, parts, table, units, length):
    return pl.pallas_call(
        functools.partial(mid_kernel, layer, length),
        out_shape=jax.ShapeDtypeStruct((parts.shape[0], units, parts.shape[2]), BF16),
        in_specs=[VMEM] * 2,
        out_specs=VMEM,
        cost_estimate=cost(1000000, parts.size * 2),
        compiler_params=room(6),
    )(parts, table)


def down_kernel(layer, start, half, ny, nx, hidden, *refs):
    out = refs[-1]
    sides = [refs[0:ny], refs[ny : 2 * ny]]
    nz, _, tokens = hidden.shape
    core = lax.axis_index("dp")
    y = lax.axis_index("y")
    term = 0.0
    for side, weights in enumerate(sides):
        first = (core if side == 0 else 1 - core) * (nz // 2)
        rows = hidden[pl.ds(first, nz // 2)].reshape(half, tokens).T
        weight = jnp.concatenate([w[pl.ds(start, half), :] for w in weights], axis=1)
        term = term + jnp.dot(rows, weight, preferred_element_type=F32)
    for k in range(ny):
        piece = term[:, k * LANES : (k + 1) * LANES]
        at = lax.rem(y - k + ny, ny)
        if layer == 0:
            out[:, at] = piece.reshape(ny * nx, -1, LANES).astype(BF16)
        else:
            for i in range(nx):
                out[at * nx + i] = piece.astype(BF16)


def lowered(layer, start, half, ny, nx, args):
    tokens = args[0].shape[2]
    count = ny * nx
    shape = (count, ny, tokens // count, LANES) if layer == 0 else (count, tokens, LANES)
    return pl.pallas_call(
        functools.partial(down_kernel, layer, start, half, ny, nx),
        out_shape=jax.ShapeDtypeStruct(shape, BF16),
        in_specs=[VMEM] * len(args),
        out_specs=VMEM,
        cost_estimate=cost(4 * half * ny * LANES * tokens, 4 * half * ny * LANES),
        compiler_params=room(8),
    )(*args)


def add_kernel(terms, mine, out):
    count, ny, piece, _ = terms.shape
    place = lax.axis_index("y") * (count // ny) + lax.axis_index("x")
    total = terms[0].astype(F32)
    for i in range(1, count):
        total = total + terms[i].astype(F32)
    rows = pl.multiple_of(place * piece, piece)
    own = mine[:, pl.ds(rows, piece), :].astype(F32)
    fresh = (0.5 * own + total).astype(BF16)
    for i in range(count):
        out[i] = fresh


def added(terms, mine):
    return pl.pallas_call(
        add_kernel,
        out_shape=jax.ShapeDtypeStruct(terms.shape, BF16),
        in_specs=[VMEM] * 2,
        out_specs=VMEM,
        cost_estimate=cost(1000000, terms.size * 4),
        compiler_params=room(4),
        name="add",
    )(terms, mine)


def last_kernel(terms, kept, last, out):
    total = terms[0].astype(F32)
    for i in range(1, terms.shape[0]):
        total = total + terms[i].astype(F32)
    fresh = (0.5 * kept[...].astype(F32) + total).astype(BF16)
    last[...] = fresh
    values = fresh.astype(F32)
    both = high_and_low(values * values)
    for i in range(out.shape[0]):
        out[i] = both


def finished(terms, kept, copies):
    return pl.pallas_call(
        last_kernel,
        out_shape=[
            jax.ShapeDtypeStruct(kept.shape, BF16),
            jax.ShapeDtypeStruct((copies, EXTRA, terms.shape[1]), BF16),
        ],
        in_specs=[VMEM] * 2,
        out_specs=[VMEM] * 2,
        cost_estimate=cost(1000000, terms.size * 4),
        compiler_params=room(4),
        name="last",
    )(terms, kept)


def norm_kernel(last, parts, gain, out):
    tokens = last.shape[0]
    total = parts[0].astype(F32)
    for i in range(1, parts.shape[0]):
        total = total + parts[i].astype(F32)
    scale = lax.rsqrt((total[0:1] + total[1:2]) / D + EPS)
    column = jnp.broadcast_to(scale, (LANES, tokens)).T
    values = last[...].astype(F32) * column * gain[...].astype(F32)
    out[...] = values.astype(BF16)


def normed(last, parts, gain):
    return pl.pallas_call(
        norm_kernel,
        out_shape=jax.ShapeDtypeStruct(last.shape, BF16),
        in_specs=[VMEM] * 3,
        out_specs=VMEM,
        cost_estimate=cost(1000000, last.size * 4),
        compiler_params=room(4),
        name="norm",
    )(last, parts, gain)


def layers(
    stream,
    norm_gain,
    gate_weight,
    value_weight,
    gate_taps,
    value_taps,
    gate_bias,
    value_bias,
    down_weight,
    final_gain,
):
    batch_rows, length, width = stream.shape
    tokens = batch_rows * length
    ny, nx, nz = lax.axis_size("y"), lax.axis_size("x"), lax.axis_size("z")
    block = gate_weight.shape[2] // ny
    half = block // 2
    units = block // nz
    start = tokens + LAYERS * 8
    swap = [(0, 1), (1, 0)]
    own = stream.reshape(tokens, width)

    mine = packed_first(ny, gate_weight, value_weight, own, norm_gain)
    mine = exchanged(mine, "y")
    other = lax.ppermute(mine, "dp", swap)
    (parts,) = first_projected(0, start, block, ny, nz, [mine])
    parts, state = first_projected(1, start, block, ny, nz, [mine, other, parts])
    parts = exchanged(parts, "z")

    later = packed_second(ny, gate_weight, value_weight, down_weight)
    ups, downs = later[: ny + 1], later[ny + 1 :]
    turns = [[(i, (i + k) % ny) for i in range(ny)] for k in range(ny)]
    near_down, near_up = [downs[0]], [ups[0]]
    for k in range(1, ny):
        near_down.append(lax.ppermute(downs[k], "y", turns[k]))
        near_up.append(lax.ppermute(ups[k], "y", turns[k]))

    lower = lax.axis_index("y") * block + lax.axis_index("z") * units
    table = jnp.concatenate(
        [gate_taps, gate_bias[:, None], value_taps, value_bias[:, None]], axis=1
    )
    table = lax.dynamic_slice_in_dim(table, lower, units, 2).astype(F32)
    table = jnp.pad(table, ((0, 0), (0, 0), (0, LANES - units)))

    hidden = gated(0, parts, table, units, length)
    hidden = exchanged(hidden, "z")
    far_down = [downs[ny]] + [lax.ppermute(piece, "dp", swap) for piece in near_down[1:]]
    lows = [*near_down, *far_down]
    terms = lowered(0, 0, half, ny, nx, [hidden, *lows])
    terms = exchanged(terms, ("y", "x"))
    far_up = [ups[ny]] + [lax.ppermute(piece, "dp", swap) for piece in near_up[1:]]
    fresh = exchanged(added(terms, state), ("y", "x"))

    parts, kept = second_projected(block, ny, nz, [state, fresh, *near_up, *far_up])
    hidden = exchanged(gated(1, exchanged(parts, "z"), table, units, length), "z")
    terms = lowered(1, half, half, ny, nx, [hidden, *lows])
    terms = exchanged(terms, ("y", "x"))
    last, squares = finished(terms, kept, nz * ny)
    squares = exchanged(squares, ("z", "y"))
    mixed = normed(last, squares, final_gain[None])
    return mixed.reshape(batch_rows, length, width)


def solution(mesh):
    split = Mesh(
        mesh.devices.reshape(8, 4, mesh.shape["cb"], mesh.shape["dp"]), ("z", "y", "x", "dp")
    )
    ra = ("z", "y")
    return jax.shard_map(
        layers,
        mesh=split,
        in_specs=(
            P("dp", None, ra),
            P(None, ra),
            P(None, ra, "x"),
            P(None, ra, "x"),
            P(None, None, "x"),
            P(None, None, "x"),
            P(None, "x"),
            P(None, "x"),
            P(None, "x", ra),
            P(ra),
        ),
        out_specs=P("dp", None, ra),
        check_vma=False,
    )
```

profile of v0, /device:TPU:2, one launch (start us, length us, event | category | flops | bytes accessed | tf_op | source)
XLA Modules:
  0.0 149.3 jit_solution(7280249422990197074)
XLA Ops:
  0.0 2.4 %pack0.1 = bf16[4,912,128]{2,1,0:T(8,128)(2,1)} custom-call(bf16[2,128,3072]{2,1,0:T(8,128)(2,1)} %gate.3, bf16[2,128,3072]{2,1,0:T(8,128)(2,1)} %value.3, bf16[128,128]{1,0:T(8,128)(2,1)} %bitcast.6, bf16[2,128]{1,0:T(2,128)(2,1)} %gain.1), custom_call_target="tpu_custom_call" | custom-call | flops 1000000 | bytes 933888 | tf_op jit(solution)/shard_map/pack0/pallas_call | solution.py:100
  2.4 18.3 %all_to_all.45.refs_0_ = bf16[4,912,128]{2,1,0:T(8,128)(2,1)S(1)} all-to-all(bf16[4,912,128]{2,1,0:T(8,128)(2,1)} %pack0.1), channel_id=1, replica_groups=mesh['z'=8,'y'=4,'x'=4,'dp'=2] {'y'}, dimensions={0} | all-to-all | bytes 1867776 | tf_op jit(solution)/shard_map/all_to_all | solution.py:25
  20.7 0.3 shard_map.100.refs_2_
  21.1 2.1 %collective-permute-done.refs_1_ = bf16[4,912,128]{2,1,0:T(8,128)(2,1)S(1)} collective-permute-done((bf16[4,912,128]{2,1,0:T(8,128)(2,1)S(1)}, bf16[4,912,128]{2,1,0:T(8,128)(2,1)S(1)}, u32[]{:S(2)}, u32[]{:S(2)}) %collective-permute-start) | collective-permute-done | bytes 933920 | tf_op jit(solution)/shard_map/ppermute | solution.py:472
  23.2 0.4 shard_map.101
  23.7 0.7 copy-done.7
  24.3 0.7 copy-done.9
  25.1 8.5 %all-to-all-start.1 = ((bf16[8,200,128]{2,1,0:T(8,128)(2,1)}), bf16[8,200,128]{2,1,0:T(8,128)(2,1)S(1)}, u32[]{:S(2)}, u32[]{:S(2)}) async-start(bf16[8,200,128]{2,1,0:T(8,128)(2,1)} %copy-done.9), calls=%async_computation.1 | async-start | bytes 819200 | tf_op jit(solution)/shard_map/all_to_all | solution.py:25
  33.6 1.4 copy-done.2
  35.0 2.9 %pack1.1 = (bf16[768,128]{1,0:T(8,128)(2,1)S(1)}, bf16[768,128]{1,0:T(8,128)(2,1)S(1)}, bf16[768,128]{1,0:T(8,128)(2,1)S(1)}, bf16[768,128]{1,0:T(8,128)(2,1)S(1...) custom-call(bf16[2,128,3072]{2,1,0:T(8,128)(2,1)S(1)} %copy-done, ...), custom_call_target="tpu_custom_call" | custom-call | flops 1000000 | bytes 786432 | tf_op jit(solution)/shard_map/pack1/pallas_call | solution.py:152
  37.8 0.7 copy-done.3
  38.5 0.7 copy-done.5
  39.2 0.7 copy-done.10
  39.9 0.7 copy-done.12
  40.5 0.7 copy-done.17
  41.2 0.7 copy-done.18
  41.9 0.7 copy-done.19
  42.6 0.6 collective-permute-start.1
  43.2 2.1 %collective-permute-start.2 = (bf16[768,128]{1,0:T(8,128)(2,1)}, bf16[768,128]{1,0:T(8,128)(2,1)S(1)}, u32[]{:S(2)}, u32[]{:S(2)}) collective-permute-start(bf16[768,128]{1,0:T(8,128)(2,1)} %get-tuple-element.25), channel_id=1, source_target_pairs={{0,16},{8,24},{16,0},{24,8},{1,17},{9,25},{17,1},{25,9},{2,18},{10... | collective-permute-start | bytes 589832 | tf_op jit(solution)/shard_map/ppermute | solution.py:482
  45.2 1.1 collective-permute-start.3
  46.4 0.7 copy.14
  47.1 0.7 copy.16
  47.8 0.8 copy.13
  48.6 0.8 copy.15
  49.5 1.0 shard_map.102
  50.5 7.3 %all-to-all-start.2 = ((bf16[8,96,128]{2,1,0:T(8,128)(2,1)}), bf16[8,96,128]{2,1,0:T(8,128)(2,1)S(1)}, u32[]{:S(2)}, u32[]{:S(2)}) async-start(bf16[8,96,128]{2,1,0:T(8,128)(2,1)} %shard_map.102), calls=%async_computation.2 | async-start | bytes 393216 | tf_op jit(solution)/shard_map/all_to_all | solution.py:25
  58.0 0.5 collective-permute-start.5
  58.5 0.1 collective-permute-start.6
  58.6 0.9 collective-permute-start.7
  59.5 1.5 %collective-permute-start.8 = (bf16[768,128]{1,0:T(8,128)(2,1)}, bf16[768,128]{1,0:T(8,128)(2,1)S(1)}, u32[]{:S(2)}, u32[]{:S(2)}) collective-permute-start(bf16[768,128]{1,0:T(8,128)(2,1)} %copy-done.18), channel_id=1, source_target_pairs={{0,16},{8,24},{16,0},{24,8},{1,17},{9,25},{17,1},{25,9},{2,18},{10... | collective-permute-start | bytes 589832 | tf_op jit(solution)/shard_map/ppermute | solution.py:483
  61.0 2.6 %collective-permute-start.9 = (bf16[768,128]{1,0:T(8,128)(2,1)}, bf16[768,128]{1,0:T(8,128)(2,1)S(1)}, u32[]{:S(2)}, u32[]{:S(2)}) collective-permute-start(bf16[768,128]{1,0:T(8,128)(2,1)} %copy-done.17), channel_id=1, source_target_pairs={{0,24},{8,0},{16,8},{24,16},{1,25},{9,1},{17,9},{25,17},{2,26},{10... | collective-permute-start | bytes 589832 | tf_op jit(solution)/shard_map/ppermute | solution.py:483
  63.6 4.0 %all-to-all-done.2.hidden = bf16[8,96,128]{2,1,0:T(8,128)(2,1)S(1)} async-done(((bf16[8,96,128]{2,1,0:T(8,128)(2,1)}), bf16[8,96,128]{2,1,0:T(8,128)(2,1)S(1)}, u32[]{:S(2)}, u32[]{:S(2)}) %all-to-all-start.2) | async-done | bytes 196640 | tf_op jit(solution)/shard_map/all_to_all | solution.py:25
  67.6 1.0 shard_map.103
  68.6 6.7 %all-to-all-start.3 = ((bf16[16,4,8,128]{3,2,1,0:T(8,128)(2,1)}), bf16[16,4,8,128]{3,2,1,0:T(8,128)(2,1)S(1)}, u32[]{:S(2)}, u32[]{:S(2)}) async-start(bf16[16,4,8,128]{3,2,1,0:T(8,128)(2,1)} %shard_map.103), calls=%async_computation.3 | async-start | bytes 262144 | tf_op jit(solution)/shard_map/all_to_all | solution.py:25
  75.4 0.5 collective-permute-start.11
  76.0 5.9 %all-to-all-done.3.terms = bf16[16,4,8,128]{3,2,1,0:T(8,128)(2,1)S(1)} async-done(((bf16[16,4,8,128]{3,2,1,0:T(8,128)(2,1)}), bf16[16,4,8,128]{3,2,1,0:T(8,128)(2,1)S(1)}, u32[]{:S(2)}, u32[]{:S(2)}) %all-to-all-start.3) | async-done | bytes 131104 | tf_op jit(solution)/shard_map/all_to_all | solution.py:25
  81.9 0.7 add.11
  82.6 4.8 %all-to-all-start.4 = ((bf16[16,4,8,128]{3,2,1,0:T(8,128)(2,1)}), bf16[16,4,8,128]{3,2,1,0:T(8,128)(2,1)S(1)}, u32[]{:S(2)}, u32[]{:S(2)}) async-start(bf16[16,4,8,128]{3,2,1,0:T(8,128)(2,1)} %add.11), calls=%async_computation.4 | async-start | bytes 262144 | tf_op jit(solution)/shard_map/all_to_all | solution.py:25
  87.4 6.7 %all-to-all-done.4.refs_1_ = bf16[16,4,8,128]{3,2,1,0:T(8,128)(2,1)S(1)} async-done(((bf16[16,4,8,128]{3,2,1,0:T(8,128)(2,1)}), bf16[16,4,8,128]{3,2,1,0:T(8,128)(2,1)S(1)}, u32[]{:S(2)}, u32[]{:S(2)}) %all-to-all-start.4) | async-done | bytes 131104 | tf_op jit(solution)/shard_map/all_to_all | solution.py:25
  94.1 0.5 up1.1
  94.6 14.4 %all_to_all.46.parts = bf16[8,200,128]{2,1,0:T(8,128)(2,1)S(1)} all-to-all(bf16[8,200,128]{2,1,0:T(8,128)(2,1)S(1)} %get-tuple-element.33), channel_id=1, replica_groups=mesh['z'=8,'y'=4,'x'=4,'dp'=2] {'z'}, dimensions={0} | all-to-all | bytes 819200 | tf_op jit(solution)/shard_map/all_to_all | solution.py:25
  109.1 0.3 shard_map.104
  109.4 12.2 %all_to_all.47.hidden = bf16[8,96,128]{2,1,0:T(8,128)(2,1)S(1)} all-to-all(bf16[8,96,128]{2,1,0:T(8,128)(2,1)S(1)} %shard_map.104), channel_id=1, replica_groups=mesh['z'=8,'y'=4,'x'=4,'dp'=2] {'z'}, dimensions={0} | all-to-all | bytes 393216 | tf_op jit(solution)/shard_map/all_to_all | solution.py:25
  121.6 0.3 shard_map.105
  121.9 13.4 %all_to_all.48.terms = bf16[16,128,128]{2,1,0:T(8,128)(2,1)S(1)} all-to-all(bf16[16,128,128]{2,1,0:T(8,128)(2,1)S(1)} %shard_map.105), channel_id=1, replica_groups=mesh['z'=8,'y'=4,'x'=4,'dp'=2] {'y','x'}, dimensions={0} | all-to-all | bytes 1048576 | tf_op jit(solution)/shard_map/all_to_all | solution.py:25
  135.3 0.2 last.1
  135.5 13.0 %all_to_all.49.parts = bf16[32,8,128]{2,1,0:T(8,128)(2,1)S(1)} all-to-all(bf16[32,8,128]{2,1,0:T(8,128)(2,1)S(1)} %get-tuple-element.36), channel_id=1, replica_groups=mesh['z'=8,'y'=4,'x'=4,'dp'=2] {'z','y'}, dimensions={0} | all-to-all | bytes 131072 | tf_op jit(solution)/shard_map/all_to_all | solution.py:25
  148.5 0.8 norm.1
  (49 shorter events, 0.5 us)
Async XLA Ops:
  20.7 2.5 %collective-permute-start = (bf16[4,912,128]{2,1,0:T(8,128)(2,1)S(1)}, bf16[4,912,128]{2,1,0:T(8,128)(2,1)S(1)}, u32[]{:S(2)}, u32[]{:S(2)}) collective-permute-start(bf16[4,912,128]{2,1,0:T(8,128)(2,1)S(1)} %all_to_all.45.refs_0_), channel_id=1, source_target_pairs={{0,1},{1,0},{2,3},{3,2},{4,5},{5,4},{6,7},{7,6},{8,9},{9,8},{10,11... | collective-permute-start | bytes 2801672 | tf_op jit(solution)/shard_map/ppermute | solution.py:472
  20.7 12.8 %copy-start.1 = (bf16[2,128,3072]{2,1,0:T(8,128)(2,1)S(1)}, bf16[2,128,3072]{2,1,0:T(8,128)(2,1)}, u32[]{:S(2)}) copy-start(bf16[2,128,3072]{2,1,0:T(8,128)(2,1)} %value.3) | copy-start | bytes 4718596
  21.1 12.5 %copy-start = (bf16[2,128,3072]{2,1,0:T(8,128)(2,1)S(1)}, bf16[2,128,3072]{2,1,0:T(8,128)(2,1)}, u32[]{:S(2)}) copy-start(bf16[2,128,3072]{2,1,0:T(8,128)(2,1)} %gate.3) | copy-start | bytes 4718596
  23.6 0.7 copy-start.7
  24.3 0.7 copy-start.9
  25.1 24.5 %all-to-all-start.1 = ((bf16[8,200,128]{2,1,0:T(8,128)(2,1)}), bf16[8,200,128]{2,1,0:T(8,128)(2,1)S(1)}, u32[]{:S(2)}, u32[]{:S(2)}) async-start(bf16[8,200,128]{2,1,0:T(8,128)(2,1)} %copy-done.9), calls=%async_computation.1 | async-start | bytes 819200 | tf_op jit(solution)/shard_map/all_to_all | solution.py:25
  33.6 1.4 copy-start.2
  37.8 0.7 copy-start.3
  38.5 0.7 copy-start.5
  39.2 0.7 copy-start.10
  39.9 0.7 copy-start.12
  40.5 0.7 copy-start.17
  41.2 0.7 copy-start.18
  41.9 0.7 copy-start.19
  42.6 25.0 %copy-start.4 = (bf16[768,128]{1,0:T(8,128)(2,1)S(1)}, bf16[768,128]{1,0:T(8,128)(2,1)}, u32[]{:S(2)}) copy-start(bf16[768,128]{1,0:T(8,128)(2,1)} %copy-done.3) | copy-start | bytes 589828
  42.6 25.0 %copy-start.6 = (bf16[768,128]{1,0:T(8,128)(2,1)S(1)}, bf16[768,128]{1,0:T(8,128)(2,1)}, u32[]{:S(2)}) copy-start(bf16[768,128]{1,0:T(8,128)(2,1)} %copy-done.5) | copy-start | bytes 589828
  42.6 15.3 %collective-permute-start.1 = (bf16[768,128]{1,0:T(8,128)(2,1)}, bf16[768,128]{1,0:T(8,128)(2,1)S(1)}, u32[]{:S(2)}, u32[]{:S(2)}) collective-permute-start(bf16[768,128]{1,0:T(8,128)(2,1)} %get-tuple-element.24), channel_id=1, source_target_pairs={{0,8},{8,16},{16,24},{24,0},{1,9},{9,17},{17,25},{25,1},{2,10},{10... | collective-permute-start | bytes 589832 | tf_op jit(solution)/shard_map/ppermute | solution.py:482
  43.2 14.8 %collective-permute-start.2 = (bf16[768,128]{1,0:T(8,128)(2,1)}, bf16[768,128]{1,0:T(8,128)(2,1)S(1)}, u32[]{:S(2)}, u32[]{:S(2)}) collective-permute-start(bf16[768,128]{1,0:T(8,128)(2,1)} %get-tuple-element.25), channel_id=1, source_target_pairs={{0,16},{8,24},{16,0},{24,8},{1,17},{9,25},{17,1},{25,9},{2,18},{10... | collective-permute-start | bytes 589832 | tf_op jit(solution)/shard_map/ppermute | solution.py:482
  45.2 13.2 %collective-permute-start.3 = (bf16[768,128]{1,0:T(8,128)(2,1)}, bf16[768,128]{1,0:T(8,128)(2,1)S(1)}, u32[]{:S(2)}, u32[]{:S(2)}) collective-permute-start(bf16[768,128]{1,0:T(8,128)(2,1)} %get-tuple-element.26), channel_id=1, source_target_pairs={{0,24},{8,0},{16,8},{24,16},{1,25},{9,1},{17,9},{25,17},{2,26},{10... | collective-permute-start | bytes 589832 | tf_op jit(solution)/shard_map/ppermute | solution.py:482
  49.5 8.3 %copy-start.14 = (f32[2,8,128]{2,1,0:T(8,128)}, f32[2,8,128]{2,1,0:T(8,128)S(1)}, u32[]{:S(2)}) copy-start(f32[2,8,128]{2,1,0:T(8,128)S(1)} %pad_convert_fusion.table) | copy-start | bytes 24580
  49.5 32.4 %copy-start.8 = (bf16[4,144,128]{2,1,0:T(8,128)(2,1)S(1)}, bf16[4,144,128]{2,1,0:T(8,128)(2,1)}, u32[]{:S(2)}) copy-start(bf16[4,144,128]{2,1,0:T(8,128)(2,1)} %copy-done.7) | copy-start | bytes 442372
  50.5 43.6 %copy-start.11 = (bf16[768,128]{1,0:T(8,128)(2,1)S(1)}, bf16[768,128]{1,0:T(8,128)(2,1)}, u32[]{:S(2)}) copy-start(bf16[768,128]{1,0:T(8,128)(2,1)} %copy-done.10) | copy-start | bytes 589828
  50.5 43.6 %copy-start.13 = (bf16[768,128]{1,0:T(8,128)(2,1)S(1)}, bf16[768,128]{1,0:T(8,128)(2,1)}, u32[]{:S(2)}) copy-start(bf16[768,128]{1,0:T(8,128)(2,1)} %copy-done.12) | copy-start | bytes 589828
  50.5 17.1 %all-to-all-start.2 = ((bf16[8,96,128]{2,1,0:T(8,128)(2,1)}), bf16[8,96,128]{2,1,0:T(8,128)(2,1)S(1)}, u32[]{:S(2)}, u32[]{:S(2)}) async-start(bf16[8,96,128]{2,1,0:T(8,128)(2,1)} %shard_map.102), calls=%async_computation.2 | async-start | bytes 393216 | tf_op jit(solution)/shard_map/all_to_all | solution.py:25
  57.9 3.1 %collective-permute-start.4 = (bf16[768,128]{1,0:T(8,128)(2,1)S(1)}, bf16[768,128]{1,0:T(8,128)(2,1)S(1)}, u32[]{:S(2)}, u32[]{:S(2)}) collective-permute-start(bf16[768,128]{1,0:T(8,128)(2,1)S(1)} %collective-permute-done.1.refs_1_), channel_id=1, source_target_pairs={{0,1},{1,0},{2,3},{3,2},{4,5},{5,4},{6,7},{7,6},{8,9},{9,8},{10,11... | collective-permute-start | bytes 589832 | tf_op jit(solution)/shard_map/ppermute | solution.py:494
  58.0 5.6 %collective-permute-start.5 = (bf16[768,128]{1,0:T(8,128)(2,1)S(1)}, bf16[768,128]{1,0:T(8,128)(2,1)S(1)}, u32[]{:S(2)}, u32[]{:S(2)}) collective-permute-start(bf16[768,128]{1,0:T(8,128)(2,1)S(1)} %collective-permute-done.2.refs_2_), channel_id=1, source_target_pairs={{0,1},{1,0},{2,3},{3,2},{4,5},{5,4},{6,7},{7,6},{8,9},{9,8},{10,11... | collective-permute-start | bytes 589832 | tf_op jit(solution)/shard_map/ppermute | solution.py:494
  58.5 5.2 %collective-permute-start.6 = (bf16[768,128]{1,0:T(8,128)(2,1)S(1)}, bf16[768,128]{1,0:T(8,128)(2,1)S(1)}, u32[]{:S(2)}, u32[]{:S(2)}) collective-permute-start(bf16[768,128]{1,0:T(8,128)(2,1)S(1)} %collective-permute-done.3.refs_3_), channel_id=1, source_target_pairs={{0,1},{1,0},{2,3},{3,2},{4,5},{5,4},{6,7},{7,6},{8,9},{9,8},{10,11... | collective-permute-start | bytes 589832 | tf_op jit(solution)/shard_map/ppermute | solution.py:494
  58.6 16.7 %collective-permute-start.7 = (bf16[768,128]{1,0:T(8,128)(2,1)}, bf16[768,128]{1,0:T(8,128)(2,1)S(1)}, u32[]{:S(2)}, u32[]{:S(2)}) collective-permute-start(bf16[768,128]{1,0:T(8,128)(2,1)} %copy-done.19), channel_id=1, source_target_pairs={{0,8},{8,16},{16,24},{24,0},{1,9},{9,17},{17,25},{25,1},{2,10},{10... | collective-permute-start | bytes 589832 | tf_op jit(solution)/shard_map/ppermute | solution.py:483
  59.5 15.9 %collective-permute-start.8 = (bf16[768,128]{1,0:T(8,128)(2,1)}, bf16[768,128]{1,0:T(8,128)(2,1)S(1)}, u32[]{:S(2)}, u32[]{:S(2)}) collective-permute-start(bf16[768,128]{1,0:T(8,128)(2,1)} %copy-done.18), channel_id=1, source_target_pairs={{0,16},{8,24},{16,0},{24,8},{1,17},{9,25},{17,1},{25,9},{2,18},{10... | collective-permute-start | bytes 589832 | tf_op jit(solution)/shard_map/ppermute | solution.py:483
  61.0 14.9 %collective-permute-start.9 = (bf16[768,128]{1,0:T(8,128)(2,1)}, bf16[768,128]{1,0:T(8,128)(2,1)S(1)}, u32[]{:S(2)}, u32[]{:S(2)}) collective-permute-start(bf16[768,128]{1,0:T(8,128)(2,1)} %copy-done.17), channel_id=1, source_target_pairs={{0,24},{8,0},{16,8},{24,16},{1,25},{9,1},{17,9},{25,17},{2,26},{10... | collective-permute-start | bytes 589832 | tf_op jit(solution)/shard_map/ppermute | solution.py:483
  68.6 13.3 %all-to-all-start.3 = ((bf16[16,4,8,128]{3,2,1,0:T(8,128)(2,1)}), bf16[16,4,8,128]{3,2,1,0:T(8,128)(2,1)S(1)}, u32[]{:S(2)}, u32[]{:S(2)}) async-start(bf16[16,4,8,128]{3,2,1,0:T(8,128)(2,1)} %shard_map.103), calls=%async_computation.3 | async-start | bytes 262144 | tf_op jit(solution)/shard_map/all_to_all | solution.py:25
  75.3 12.1 %collective-permute-start.10 = (bf16[768,128]{1,0:T(8,128)(2,1)S(1)}, bf16[768,128]{1,0:T(8,128)(2,1)S(1)}, u32[]{:S(2)}, u32[]{:S(2)}) collective-permute-start(bf16[768,128]{1,0:T(8,128)(2,1)S(1)} %collective-permute-done.7.refs_3_), channel_id=1, source_target_pairs={{0,1},{1,0},{2,3},{3,2},{4,5},{5,4},{6,7},{7,6},{8,9},{9,8},{10,11... | collective-permute-start | bytes 589832 | tf_op jit(solution)/shard_map/ppermute | solution.py:498
  75.4 12.0 %collective-permute-start.11 = (bf16[768,128]{1,0:T(8,128)(2,1)S(1)}, bf16[768,128]{1,0:T(8,128)(2,1)S(1)}, u32[]{:S(2)}, u32[]{:S(2)}) collective-permute-start(bf16[768,128]{1,0:T(8,128)(2,1)S(1)} %collective-permute-done.8.refs_4_), channel_id=1, source_target_pairs={{0,1},{1,0},{2,3},{3,2},{4,5},{5,4},{6,7},{7,6},{8,9},{9,8},{10,11... | collective-permute-start | bytes 589832 | tf_op jit(solution)/shard_map/ppermute | solution.py:498
  75.9 11.5 %collective-permute-start.12 = (bf16[768,128]{1,0:T(8,128)(2,1)S(1)}, bf16[768,128]{1,0:T(8,128)(2,1)S(1)}, u32[]{:S(2)}, u32[]{:S(2)}) collective-permute-start(bf16[768,128]{1,0:T(8,128)(2,1)S(1)} %collective-permute-done.9.refs_5_), channel_id=1, source_target_pairs={{0,1},{1,0},{2,3},{3,2},{4,5},{5,4},{6,7},{7,6},{8,9},{9,8},{10,11... | collective-permute-start | bytes 589832 | tf_op jit(solution)/shard_map/ppermute | solution.py:498
  81.9 27.1 %copy-start.15 = (f32[2,8,128]{2,1,0:T(8,128)S(1)}, f32[2,8,128]{2,1,0:T(8,128)}, u32[]{:S(2)}) copy-start(f32[2,8,128]{2,1,0:T(8,128)} %copy-done.14) | copy-start | bytes 24580
  82.6 11.5 %all-to-all-start.4 = ((bf16[16,4,8,128]{3,2,1,0:T(8,128)(2,1)}), bf16[16,4,8,128]{3,2,1,0:T(8,128)(2,1)S(1)}, u32[]{:S(2)}, u32[]{:S(2)}) async-start(bf16[16,4,8,128]{3,2,1,0:T(8,128)(2,1)} %add.11), calls=%async_computation.4 | async-start | bytes 262144 | tf_op jit(solution)/shard_map/all_to_all | solution.py:25
  121.5 27.0 %copy-start.16 = (bf16[128]{0:T(256)(128)(2,1)S(1)}, bf16[128]{0:T(256)(128)(2,1)}, u32[]{:S(2)}) copy-start(bf16[128]{0:T(256)(128)(2,1)} %param.19) | copy-start | bytes 772
where the time goes:
time: 150 us; the launch traced here: 149 us
  blocking collectives  71.4 us (48%)
  starting transfers between devices  37.4 us (25%)
  waiting for transfers between devices  18.8 us (13%)
  Pallas kernels  10.8 us (7%)
  local copies, waits for them, and re-layouts  10.6 us (7%)
    all_to_all x5, blocking collectives, exchanged(): return lax.all_to_all(x, axis, split_axis=0, concat_axis=0, tiled=True)  71.4 us
    all_to_all x4, starting transfers between devices, exchanged(): return lax.all_to_all(x, axis, split_axis=0, concat_axis=0, tiled=True)  27.2 us
    all_to_all x4, waiting for transfers between devices, exchanged(): return lax.all_to_all(x, axis, split_axis=0, concat_axis=0, tiled=True)  16.6 us
    unnamed x42, local copies, waits for them, and re-layouts  9.19 us
    ppermute x3, starting transfers between devices, layers(): near_up.append(lax.ppermute(ups[k], 'y', turns[k]))  5.04 us
    ppermute x3, starting transfers between devices, layers(): near_down.append(lax.ppermute(downs[k], 'y', turns[k]))  3.76 us
  transfers between devices with their start and end apart: 17, of which 4 were waited for; matrix products, arithmetic and copies ran while one was open for 2% of the time, Pallas kernels for 4%

commit v1 on v0

--- a/solution.py
+++ b/solution.py
@@ -118,6 +118,7 @@
 def pack_second_kernel(ny, gate, value, down, *refs):
     outs, sems = refs[:-1], refs[-1]
     ups = gate.shape[2] // ny // LANES
+    rows = ups * gate.shape[1]
     each = ups + LAYERS
     core = lax.axis_index("dp")
     y = lax.axis_index("y")
@@ -128,8 +129,7 @@
             side = core if k < ny else 1 - core
             first = k * each
             yield from up_copies(up if k < ny else spare, 1, ny, at, outs[k], 0, sems, first)
-            low = outs[ny + 1 + k]
-            yield from down_copies(down, ny, side, at, low, 0, sems, first + ups)
+            yield from down_copies(down, ny, side, at, outs[k], rows, sems, first + ups)
 
     @pl.when(core == 0)
     def _():
@@ -146,15 +146,13 @@
 
 
 def packed_second(ny, gate, value, down):
-    rows = gate.shape[1] * gate.shape[2] // ny // LANES
-    low = LAYERS * down.shape[1] // ny // 2
+    rows = gate.shape[1] * gate.shape[2] // ny // LANES + LAYERS * down.shape[1] // ny // 2
     each = gate.shape[2] // ny // LANES + LAYERS
     return pl.pallas_call(
         functools.partial(pack_second_kernel, ny),
-        out_shape=[jax.ShapeDtypeStruct((rows, LANES), BF16)] * (ny + 1)
-        + [jax.ShapeDtypeStruct((low, LANES), BF16)] * (ny + 1),
+        out_shape=[jax.ShapeDtypeStruct((rows, LANES), BF16)] * (ny + 1),
         in_specs=[HBM] * 3,
-        out_specs=[VMEM] * (2 * ny + 2),
+        out_specs=[VMEM] * (ny + 1),
         scratch_shapes=[pltpu.SemaphoreType.DMA(((ny + 1) * each,))],
         cost_estimate=cost(1000000, 2 * ny * rows * LANES),
         compiler_params=room(4),
@@ -475,32 +473,27 @@
     parts = exchanged(parts, "z")
 
     later = packed_second(ny, gate_weight, value_weight, down_weight)
-    ups, downs = later[: ny + 1], later[ny + 1 :]
-    turns = [[(i, (i + k) % ny) for i in range(ny)] for k in range(ny)]
-    near_down, near_up = [downs[0]], [ups[0]]
-    for k in range(1, ny):
-        near_down.append(lax.ppermute(downs[k], "y", turns[k]))
-        near_up.append(lax.ppermute(ups[k], "y", turns[k]))
-
     lower = lax.axis_index("y") * block + lax.axis_index("z") * units
     table = jnp.concatenate(
         [gate_taps, gate_bias[:, None], value_taps, value_bias[:, None]], axis=1
     )
     table = lax.dynamic_slice_in_dim(table, lower, units, 2).astype(F32)
     table = jnp.pad(table, ((0, 0), (0, 0), (0, LANES - units)))
+    *later, table = lax.optimization_barrier((*later, table))
+    near = [later[0]]
+    for k in range(1, ny):
+        near.append(lax.ppermute(later[k], "y", [(i, (i + k) % ny) for i in range(ny)]))
 
     hidden = gated(0, parts, table, units, length)
     hidden = exchanged(hidden, "z")
-    far_down = [downs[ny]] + [lax.ppermute(piece, "dp", swap) for piece in near_down[1:]]
-    lows = [*near_down, *far_down]
-    terms = lowered(0, 0, half, ny, nx, [hidden, *lows])
+    far = [later[ny]] + [lax.ppermute(piece, "dp", swap) for piece in near[1:]]
+    terms = lowered(0, block, half, ny, nx, [hidden, *near, *far])
     terms = exchanged(terms, ("y", "x"))
-    far_up = [ups[ny]] + [lax.ppermute(piece, "dp", swap) for piece in near_up[1:]]
     fresh = exchanged(added(terms, state), ("y", "x"))
 
-    parts, kept = second_projected(block, ny, nz, [state, fresh, *near_up, *far_up])
+    parts, kept = second_projected(block, ny, nz, [state, fresh, *near, *far])
     hidden = exchanged(gated(1, exchanged(parts, "z"), table, units, length), "z")
-    terms = lowered(1, half, half, ny, nx, [hidden, *lows])
+    terms = lowered(1, block + half, half, ny, nx, [hidden, *near, *far])
     terms = exchanged(terms, ("y", "x"))
     last, squares = finished(terms, kept, nz * ny)
     squares = exchanged(squares, ("z", "y"))

time: 150 us -> 164 us (1.093)
  blocking collectives: 71.4 us -> 96.6 us
  starting transfers between devices: 37.4 us -> 19.9 us
  waiting for transfers between devices: 18.8 us -> 30.1 us
  local copies, waits for them, and re-layouts: 10.6 us -> 6.4 us
    all_to_all x5 -> x7, blocking collectives: 71.4 us -> 96.6 us  [exchanged(): return lax.all_to_all(x, axis, split_axis=0, concat_axis=0, tiled=True)]
    ppermute x12 -> x6, waiting for transfers between devices: 0.03 us -> 16.9 us  [the longest x3 16.9 us: layers(): lax.ppermute(later[k], 'y', [(i, (i + k) % ny) for i in range(ny)])]
    all_to_all x4 -> x2, starting transfers between devices: 27.2 us -> 15.5 us  [exchanged(): return lax.all_to_all(x, axis, split_axis=0, concat_axis=0, tiled=True)]
    ppermute x12 -> x6, starting transfers between devices: 10.2 us -> 4.34 us  [the longest x3 3.83 us: layers(): lax.ppermute(later[k], 'y', [(i, (i + k) % ny) for i in range(ny)])]
    all_to_all x4 -> x2, waiting for transfers between devices: 16.6 us -> 11.1 us  [exchanged(): return lax.all_to_all(x, axis, split_axis=0, concat_axis=0, tiled=True)]
    unnamed x42 -> x36, local copies, waits for them, and re-layouts: 9.19 us -> 5.13 us
  transfers between devices with their start and end apart: 17 -> 9, of which waited for: 4 -> 4; matrix products, arithmetic and copies ran while one was open for 2% -> 2% of each run, Pallas kernels for 4% -> 3%
where the time goes in v1:
time: 164 us
  blocking collectives  96.6 us (59%)
  waiting for transfers between devices  30.1 us (18%)
  starting transfers between devices  19.9 us (12%)
  Pallas kernels  10.5 us (6%)
  local copies, waits for them, and re-layouts  6.4 us (4%)
    all_to_all x7, blocking collectives, exchanged(): return lax.all_to_all(x, axis, split_axis=0, concat_axis=0, tiled=True)  96.6 us
    ppermute x3, waiting for transfers between devices, layers(): lax.ppermute(later[k], 'y', [(i, (i + k) % ny) for i in range(ny)])  16.9 us
    all_to_all x2, starting transfers between devices, exchanged(): return lax.all_to_all(x, axis, split_axis=0, concat_axis=0, tiled=True)  15.5 us
    all_to_all x2, waiting for transfers between devices, exchanged(): return lax.all_to_all(x, axis, split_axis=0, concat_axis=0, tiled=True)  11.1 us
    unnamed x36, local copies, waits for them, and re-layouts  5.13 us
    ppermute x3, starting transfers between devices, layers(): lax.ppermute(later[k], 'y', [(i, (i + k) % ny) for i in range(ny)])  3.83 us
  transfers between devices with their start and end apart: 9, of which 4 were waited for; matrix products, arithmetic and copies ran while one was open for 2% of the time, Pallas kernels for 3%

profile of v1, /device:TPU:2, one launch (start us, length us, event | category | flops | bytes accessed | tf_op | source)
XLA Modules:
  0.0 163.7 jit_solution(7044525998286189064)
XLA Ops:
  0.0 2.4 %pack0.1 = bf16[4,912,128]{2,1,0:T(8,128)(2,1)} custom-call(bf16[2,128,3072]{2,1,0:T(8,128)(2,1)} %gate.3, bf16[2,128,3072]{2,1,0:T(8,128)(2,1)} %value.3, bf16[128,128]{1,0:T(8,128)(2,1)} %bitcast.6, bf16[2,128]{1,0:T(2,128)(2,1)} %gain.1), custom_call_target="tpu_custom_call" | custom-call | flops 1000000 | bytes 933888 | tf_op jit(solution)/shard_map/pack0/pallas_call | solution.py:100
  2.4 18.4 %all_to_all.45.refs_0_ = bf16[4,912,128]{2,1,0:T(8,128)(2,1)S(1)} all-to-all(bf16[4,912,128]{2,1,0:T(8,128)(2,1)} %pack0.1), channel_id=1, replica_groups=mesh['z'=8,'y'=4,'x'=4,'dp'=2] {'y'}, dimensions={0} | all-to-all | bytes 1867776 | tf_op jit(solution)/shard_map/all_to_all | solution.py:25
  20.7 0.0 collective-permute-start
  20.8 0.0 copy-start.14
  20.8 0.3 shard_map.100.refs_2_
  21.1 0.0 copy-start
  21.1 0.0 copy-start.1
  21.1 2.1 %collective-permute-done.refs_1_ = bf16[4,912,128]{2,1,0:T(8,128)(2,1)S(1)} collective-permute-done((bf16[4,912,128]{2,1,0:T(8,128)(2,1)S(1)}, bf16[4,912,128]{2,1,0:T(8,128)(2,1)S(1)}, u32[]{:S(2)}, u32[]{:S(2)}) %collective-permute-start) | collective-permute-done | bytes 933920 | tf_op jit(solution)/shard_map/ppermute | solution.py:470
  23.2 1.2 shard_map.101
  24.5 0.7 copy-done.6
  25.1 8.5 %all-to-all-start.1 = ((bf16[8,200,128]{2,1,0:T(8,128)(2,1)}), bf16[8,200,128]{2,1,0:T(8,128)(2,1)}, u32[]{:S(2)}, u32[]{:S(2)}) async-start(bf16[8,200,128]{2,1,0:T(8,128)(2,1)} %get-tuple-element.23), calls=%async_computation.1 | async-start | bytes 819200 | tf_op jit(solution)/shard_map/all_to_all | solution.py:25
  33.6 0.6 copy.14
  34.2 0.6 copy.16
  34.9 0.6 copy.13
  35.5 0.6 copy.15
  36.1 1.4 copy-done.5
  37.5 2.1 %pack1.1 = (bf16[1536,128]{1,0:T(8,128)(2,1)S(1)}, bf16[1536,128]{1,0:T(8,128)(2,1)S(1)}, bf16[1536,128]{1,0:T(8,128)(2,1)S(1)}, bf16[1536,128]{1,0:T(8,128)(2,1)S(1)}, bf16[1536,128]{1,0:T(8,128)(2,1)S(1)}) custom-call(bf16[2,128,3072]{2,1,0:T(8,128)(2,1)S(1)} %copy-done, bf16[2,128,3072]{2,1,0:T(8,128)(2,1)S(1)} %copy-done.1, ...), custom_call_target="tpu_custom_call" | custom-call | flops 1000000 | bytes 1572864 | tf_op jit(solution)/shard_map/pack1/pallas_call | solution.py:151
  39.6 0.8 copy-done.2
  40.4 0.1 fusion.2
  40.5 0.6 collective-permute-start.1
  41.1 2.1 %collective-permute-start.2 = (bf16[1536,128]{1,0:T(8,128)(2,1)S(1)}, bf16[1536,128]{1,0:T(8,128)(2,1)S(1)}, u32[]{:S(2)}, u32[]{:S(2)}) collective-permute-start(bf16[1536,128]{1,0:T(8,128)(2,1)S(1)} %get-tuple-element.32), channel_id=1, source_target_pairs={{0,16},{8,24},{16,0},{24,8},{1,17},{9,25},{17,1},{25,9},{2,18},{10... | collective-permute-start | bytes 1179656 | tf_op jit(solution)/shard_map/ppermute | solution.py:485
  43.2 1.1 collective-permute-start.3
  44.3 16.7 %collective-permute-done.1.refs_1_.refs_3_ = bf16[1536,128]{1,0:T(8,128)(2,1)S(1)} collective-permute-done((bf16[1536,128]{1,0:T(8,128)(2,1)S(1)}, bf16[1536,128]{1,0:T(8,128)(2,1)S(1)}, u32[]{:S(2)}, u32[]{:S(2)}) %collective-permute-start.1) | collective-permute-done | bytes 393248 | tf_op jit(solution)/shard_map/ppermute | solution.py:485
  61.1 0.0 collective-permute-start.4
  61.1 0.0 collective-permute-done.2.refs_2_.refs_4_
  61.1 0.5 collective-permute-start.5
  61.6 0.1 collective-permute-done.3.refs_3_.refs_5_
  61.7 0.0 collective-permute-start.6
  61.7 0.0 all-to-all-done.1.parts
  61.7 2.1 %shard_map.102 = bf16[8,96,128]{2,1,0:T(8,128)(2,1)} custom-call(bf16[8,200,128]{2,1,0:T(8,128)(2,1)} %all-to-all-done.1.parts, f32[2,8,128]{2,1,0:T(8,128)S(1)} %pad_convert_fusion.table), custom_call_target="tpu_custom_call" | custom-call | flops 1000000 | bytes 409600 | tf_op jit(solution)/shard_map/pallas_call | solution.py:325
  63.8 7.1 %all-to-all-start.2 = ((bf16[8,96,128]{2,1,0:T(8,128)(2,1)}), bf16[8,96,128]{2,1,0:T(8,128)(2,1)S(1)}, u32[]{:S(2)}, u32[]{:S(2)}) async-start(bf16[8,96,128]{2,1,0:T(8,128)(2,1)} %shard_map.102), calls=%async_computation.2 | async-start | bytes 393216 | tf_op jit(solution)/shard_map/all_to_all | solution.py:25
  70.8 0.0 collective-permute-done.4.refs_5_.refs_7_
  70.8 0.0 collective-permute-done.5.refs_6_.refs_8_
  70.9 11.1 %all-to-all-done.2.hidden = bf16[8,96,128]{2,1,0:T(8,128)(2,1)S(1)} async-done(((bf16[8,96,128]{2,1,0:T(8,128)(2,1)}), bf16[8,96,128]{2,1,0:T(8,128)(2,1)S(1)}, u32[]{:S(2)}, u32[]{:S(2)}) %all-to-all-start.2) | async-done | bytes 196640 | tf_op jit(solution)/shard_map/all_to_all | solution.py:25
  82.0 1.0 copy-done.3
  83.0 0.3 shard_map.103
  83.3 13.3 %all_to_all.46.terms = bf16[16,4,8,128]{3,2,1,0:T(8,128)(2,1)S(1)} all-to-all(bf16[16,4,8,128]{3,2,1,0:T(8,128)(2,1)S(1)} %shard_map.103), channel_id=1, replica_groups=mesh['z'=8,'y'=4,'x'=4,'dp'=2] {'y','x'}, dimensions={0} | all-to-all | bytes 262144 | tf_op jit(solution)/shard_map/all_to_all | solution.py:25
  96.6 11.1 %all_to_all.47.refs_1_ = bf16[16,4,8,128]{3,2,1,0:T(8,128)(2,1)S(1)} all-to-all(bf16[16,4,8,128]{3,2,1,0:T(8,128)(2,1)S(1)} %add.11), channel_id=1, replica_groups=mesh['z'=8,'y'=4,'x'=4,'dp'=2] {'y','x'}, dimensions={0} | all-to-all | bytes 262144 | tf_op jit(solution)/shard_map/all_to_all | solution.py:25
  107.7 0.5 up1.1
  108.2 15.2 %all_to_all.48.parts = bf16[8,200,128]{2,1,0:T(8,128)(2,1)S(1)} all-to-all(bf16[8,200,128]{2,1,0:T(8,128)(2,1)S(1)} %get-tuple-element.35), channel_id=1, replica_groups=mesh['z'=8,'y'=4,'x'=4,'dp'=2] {'z'}, dimensions={0} | all-to-all | bytes 819200 | tf_op jit(solution)/shard_map/all_to_all | solution.py:25
  123.4 0.3 shard_map.104
  123.7 12.2 %all_to_all.49.hidden = bf16[8,96,128]{2,1,0:T(8,128)(2,1)S(1)} all-to-all(bf16[8,96,128]{2,1,0:T(8,128)(2,1)S(1)} %shard_map.104), channel_id=1, replica_groups=mesh['z'=8,'y'=4,'x'=4,'dp'=2] {'z'}, dimensions={0} | all-to-all | bytes 393216 | tf_op jit(solution)/shard_map/all_to_all | solution.py:25
  135.9 0.3 shard_map.105
  136.2 0.0 copy-start.8
  136.3 13.5 %all_to_all.50.terms = bf16[16,128,128]{2,1,0:T(8,128)(2,1)S(1)} all-to-all(bf16[16,128,128]{2,1,0:T(8,128)(2,1)S(1)} %shard_map.105), channel_id=1, replica_groups=mesh['z'=8,'y'=4,'x'=4,'dp'=2] {'y','x'}, dimensions={0} | all-to-all | bytes 1048576 | tf_op jit(solution)/shard_map/all_to_all | solution.py:25
  149.7 0.2 last.1
  149.9 13.0 %all_to_all.51.parts = bf16[32,8,128]{2,1,0:T(8,128)(2,1)S(1)} all-to-all(bf16[32,8,128]{2,1,0:T(8,128)(2,1)S(1)} %get-tuple-element.38), channel_id=1, replica_groups=mesh['z'=8,'y'=4,'x'=4,'dp'=2] {'z','y'}, dimensions={0} | all-to-all | bytes 131072 | tf_op jit(solution)/shard_map/all_to_all | solution.py:25
  162.9 0.8 norm.1
  (29 shorter events, 0.1 us)
Async XLA Ops:
  20.7 2.5 %collective-permute-start = (bf16[4,912,128]{2,1,0:T(8,128)(2,1)S(1)}, bf16[4,912,128]{2,1,0:T(8,128)(2,1)S(1)}, u32[]{:S(2)}, u32[]{:S(2)}) collective-permute-start(bf16[4,912,128]{2,1,0:T(8,128)(2,1)S(1)} %all_to_all.45.refs_0_), channel_id=1, source_target_pairs={{0,1},{1,0},{2,3},{3,2},{4,5},{5,4},{6,7},{7,6},{8,9},{9,8},{10,11... | collective-permute-start | bytes 2801672 | tf_op jit(solution)/shard_map/ppermute | solution.py:470
  20.7 12.8 %copy-start.15 = (bf16[2,3072]{1,0:T(2,128)(2,1)S(1)}, bf16[2,3072]{1,0:T(2,128)(2,1)}, u32[]{:S(2)}) copy-start(bf16[2,3072]{1,0:T(2,128)(2,1)} %param.16) | copy-start | bytes 36868
  20.7 13.5 %copy-start.16 = (bf16[2,3072]{1,0:T(2,128)(2,1)S(1)}, bf16[2,3072]{1,0:T(2,128)(2,1)}, u32[]{:S(2)}) copy-start(bf16[2,3072]{1,0:T(2,128)(2,1)} %param.17) | copy-start | bytes 36868
  20.8 14.1 %copy-start.13 = (bf16[2,3,3072]{2,0,1:T(2,128)(2,1)S(1)}, bf16[2,3,3072]{2,0,1:T(2,128)(2,1)}, u32[]{:S(2)}) copy-start(bf16[2,3,3072]{2,0,1:T(2,128)(2,1)} %param.14) | copy-start | bytes 110596
  20.8 14.7 %copy-start.14 = (bf16[2,3,3072]{2,0,1:T(2,128)(2,1)S(1)}, bf16[2,3,3072]{2,0,1:T(2,128)(2,1)}, u32[]{:S(2)}) copy-start(bf16[2,3,3072]{2,0,1:T(2,128)(2,1)} %param.15) | copy-start | bytes 110596
  21.1 15.0 %copy-start = (bf16[2,128,3072]{2,1,0:T(8,128)(2,1)S(1)}, bf16[2,128,3072]{2,1,0:T(8,128)(2,1)}, u32[]{:S(2)}) copy-start(bf16[2,128,3072]{2,1,0:T(8,128)(2,1)} %gate.3) | copy-start | bytes 4718596
  21.1 15.0 %copy-start.1 = (bf16[2,128,3072]{2,1,0:T(8,128)(2,1)S(1)}, bf16[2,128,3072]{2,1,0:T(8,128)(2,1)}, u32[]{:S(2)}) copy-start(bf16[2,128,3072]{2,1,0:T(8,128)(2,1)} %value.3) | copy-start | bytes 4718596
  24.5 0.7 copy-start.6
  25.1 36.6 %all-to-all-start.1 = ((bf16[8,200,128]{2,1,0:T(8,128)(2,1)}), bf16[8,200,128]{2,1,0:T(8,128)(2,1)}, u32[]{:S(2)}, u32[]{:S(2)}) async-start(bf16[8,200,128]{2,1,0:T(8,128)(2,1)} %get-tuple-element.23), calls=%async_computation.1 | async-start | bytes 819200 | tf_op jit(solution)/shard_map/all_to_all | solution.py:25
  36.1 1.4 copy-start.5
  37.5 2.9 %copy-start.9 = (bf16[2,3,3072]{2,1,0:T(4,128)(2,1)S(1)}, bf16[2,3,3072]{2,1,0:T(4,128)(2,1)}, u32[]{:S(2)}) copy-start(bf16[2,3,3072]{2,1,0:T(4,128)(2,1)} %copy.13) | copy-start | bytes 110596
  37.5 2.9 %copy-start.10 = (bf16[2,3,3072]{2,1,0:T(4,128)(2,1)S(1)}, bf16[2,3,3072]{2,1,0:T(4,128)(2,1)}, u32[]{:S(2)}) copy-start(bf16[2,3,3072]{2,1,0:T(4,128)(2,1)} %copy.15) | copy-start | bytes 110596
  37.5 2.9 %copy-start.11 = (bf16[2,1,3072]{2,1,0:T(2,128)(2,1)S(1)}, bf16[2,1,3072]{2,1,0:T(2,128)(2,1)}, u32[]{:S(2)}) copy-start(bf16[2,1,3072]{2,1,0:T(2,128)(2,1)} %copy.14) | copy-start | bytes 36868
  37.5 2.9 %copy-start.12 = (bf16[2,1,3072]{2,1,0:T(2,128)(2,1)S(1)}, bf16[2,1,3072]{2,1,0:T(2,128)(2,1)}, u32[]{:S(2)}) copy-start(bf16[2,1,3072]{2,1,0:T(2,128)(2,1)} %copy.16) | copy-start | bytes 36868
  39.6 0.8 copy-start.2
  40.5 20.6 %collective-permute-start.1 = (bf16[1536,128]{1,0:T(8,128)(2,1)S(1)}, bf16[1536,128]{1,0:T(8,128)(2,1)S(1)}, u32[]{:S(2)}, u32[]{:S(2)}) collective-permute-start(bf16[1536,128]{1,0:T(8,128)(2,1)S(1)} %get-tuple-element.31), channel_id=1, source_target_pairs={{0,8},{8,16},{16,24},{24,0},{1,9},{9,17},{17,25},{25,1},{2,10},{10... | collective-permute-start | bytes 1179656 | tf_op jit(solution)/shard_map/ppermute | solution.py:485
  41.1 20.0 %collective-permute-start.2 = (bf16[1536,128]{1,0:T(8,128)(2,1)S(1)}, bf16[1536,128]{1,0:T(8,128)(2,1)S(1)}, u32[]{:S(2)}, u32[]{:S(2)}) collective-permute-start(bf16[1536,128]{1,0:T(8,128)(2,1)S(1)} %get-tuple-element.32), channel_id=1, source_target_pairs={{0,16},{8,24},{16,0},{24,8},{1,17},{9,25},{17,1},{25,9},{2,18},{10... | collective-permute-start | bytes 1179656 | tf_op jit(solution)/shard_map/ppermute | solution.py:485
  43.2 18.5 %collective-permute-start.3 = (bf16[1536,128]{1,0:T(8,128)(2,1)S(1)}, bf16[1536,128]{1,0:T(8,128)(2,1)S(1)}, u32[]{:S(2)}, u32[]{:S(2)}) collective-permute-start(bf16[1536,128]{1,0:T(8,128)(2,1)S(1)} %get-tuple-element.33), channel_id=1, source_target_pairs={{0,24},{8,0},{16,8},{24,16},{1,25},{9,1},{17,9},{25,17},{2,26},{10... | collective-permute-start | bytes 1179656 | tf_op jit(solution)/shard_map/ppermute | solution.py:485
  61.1 9.8 %collective-permute-start.4 = (bf16[1536,128]{1,0:T(8,128)(2,1)S(1)}, bf16[1536,128]{1,0:T(8,128)(2,1)S(1)}, u32[]{:S(2)}, u32[]{:S(2)}) collective-permute-start(bf16[1536,128]{1,0:T(8,128)(2,1)S(1)} %collective-permute-done.1.refs_1_.refs_3_), channel_id=1, source_target_pairs={{0,1},{1,0},{2,3},{3,2},{4,5},{5,4},{6,7},{7,6},{8,9},{9,8},{10,11... | collective-permute-start | bytes 1179656 | tf_op jit(solution)/shard_map/ppermute | solution.py:489
  61.1 9.8 %collective-permute-start.5 = (bf16[1536,128]{1,0:T(8,128)(2,1)S(1)}, bf16[1536,128]{1,0:T(8,128)(2,1)S(1)}, u32[]{:S(2)}, u32[]{:S(2)}) collective-permute-start(bf16[1536,128]{1,0:T(8,128)(2,1)S(1)} %collective-permute-done.2.refs_2_.refs_4_), channel_id=1, source_target_pairs={{0,1},{1,0},{2,3},{3,2},{4,5},{5,4},{6,7},{7,6},{8,9},{9,8},{10,11... | collective-permute-start | bytes 1179656 | tf_op jit(solution)/shard_map/ppermute | solution.py:489
  61.7 9.1 %collective-permute-start.6 = (bf16[1536,128]{1,0:T(8,128)(2,1)S(1)}, bf16[1536,128]{1,0:T(8,128)(2,1)S(1)}, u32[]{:S(2)}, u32[]{:S(2)}) collective-permute-start(bf16[1536,128]{1,0:T(8,128)(2,1)S(1)} %collective-permute-done.3.refs_3_.refs_5_), channel_id=1, source_target_pairs={{0,1},{1,0},{2,3},{3,2},{4,5},{5,4},{6,7},{7,6},{8,9},{9,8},{10,11... | collective-permute-start | bytes 1179656 | tf_op jit(solution)/shard_map/ppermute | solution.py:489
  61.7 34.9 %copy-start.7 = (bf16[4,144,128]{2,1,0:T(8,128)(2,1)S(1)}, bf16[4,144,128]{2,1,0:T(8,128)(2,1)}, u32[]{:S(2)}) copy-start(bf16[4,144,128]{2,1,0:T(8,128)(2,1)} %copy-done.6) | copy-start | bytes 442372
  63.8 43.9 %copy-start.4 = (bf16[1536,128]{1,0:T(8,128)(2,1)S(1)}, bf16[1536,128]{1,0:T(8,128)(2,1)}, u32[]{:S(2)}) copy-start(bf16[1536,128]{1,0:T(8,128)(2,1)} %copy-done.2) | copy-start | bytes 1179652
  63.8 18.2 %all-to-all-start.2 = ((bf16[8,96,128]{2,1,0:T(8,128)(2,1)}), bf16[8,96,128]{2,1,0:T(8,128)(2,1)S(1)}, u32[]{:S(2)}, u32[]{:S(2)}) async-start(bf16[8,96,128]{2,1,0:T(8,128)(2,1)} %shard_map.102), calls=%async_computation.2 | async-start | bytes 393216 | tf_op jit(solution)/shard_map/all_to_all | solution.py:25
  82.0 1.0 copy-start.3
  136.2 26.7 %copy-start.8 = (bf16[128]{0:T(256)(128)(2,1)S(1)}, bf16[128]{0:T(256)(128)(2,1)}, u32[]{:S(2)}) copy-start(bf16[128]{0:T(256)(128)(2,1)} %param.19) | copy-start | bytes 772

commit v2 on v1

--- a/solution.py
+++ b/solution.py
@@ -368,6 +368,55 @@
     )(*args)
 
 
+def half_kernel(start, half, ny, hidden, *refs):
+    weights, out = refs[:ny], refs[ny]
+    nz, _, tokens = hidden.shape
+    core = lax.axis_index("dp")
+    rows = hidden[pl.ds(core * (nz // 2), nz // 2)].reshape(half, tokens).T
+    weight = jnp.concatenate([w[pl.ds(start, half), :] for w in weights], axis=1)
+    out[...] = jnp.dot(rows, weight, preferred_element_type=F32)
+
+
+def half_lowered(start, half, ny, args):
+    tokens = args[0].shape[2]
+    return pl.pallas_call(
+        functools.partial(half_kernel, start, half, ny),
+        out_shape=jax.ShapeDtypeStruct((tokens, ny * LANES), F32),
+        in_specs=[VMEM] * len(args),
+        out_specs=VMEM,
+        cost_estimate=cost(2 * half * ny * LANES * tokens, 2 * half * ny * LANES),
+        compiler_params=room(8),
+        name="down00",
+    )(*args)
+
+
+def rest_kernel(start, half, ny, nx, hidden, term, *refs):
+    weights, out = refs[:ny], refs[ny]
+    nz, _, tokens = hidden.shape
+    core = lax.axis_index("dp")
+    y = lax.axis_index("y")
+    rows = hidden[pl.ds((1 - core) * (nz // 2), nz // 2)].reshape(half, tokens).T
+    weight = jnp.concatenate([w[pl.ds(start, half), :] for w in weights], axis=1)
+    total = term[...] + jnp.dot(rows, weight, preferred_element_type=F32)
+    for k in range(ny):
+        piece = total[:, k * LANES : (k + 1) * LANES]
+        out[:, lax.rem(y - k + ny, ny)] = piece.reshape(ny * nx, -1, LANES).astype(BF16)
+
+
+def rest_lowered(start, half, ny, nx, args):
+    tokens = args[0].shape[2]
+    count = ny * nx
+    return pl.pallas_call(
+        functools.partial(rest_kernel, start, half, ny, nx),
+        out_shape=jax.ShapeDtypeStruct((count, ny, tokens // count, LANES), BF16),
+        in_specs=[VMEM] * len(args),
+        out_specs=VMEM,
+        cost_estimate=cost(2 * half * ny * LANES * tokens, 2 * half * ny * LANES),
+        compiler_params=room(8),
+        name="down01",
+    )(*args)
+
+
 def add_kernel(terms, mine, out):
     count, ny, piece, _ = terms.shape
     place = lax.axis_index("y") * (count // ny) + lax.axis_index("x")
@@ -487,7 +536,8 @@
     hidden = gated(0, parts, table, units, length)
     hidden = exchanged(hidden, "z")
     far = [later[ny]] + [lax.ppermute(piece, "dp", swap) for piece in near[1:]]
-    terms = lowered(0, block, half, ny, nx, [hidden, *near, *far])
+    terms = half_lowered(block, half, ny, [hidden, *near])
+    terms = rest_lowered(block, half, ny, nx, [hidden, terms, *far])
     terms = exchanged(terms, ("y", "x"))
     fresh = exchanged(added(terms, state), ("y", "x"))
 

time: 164 us -> 163 us (level)
  blocking collectives: 96.6 us -> 114 us
  waiting for transfers between devices: 30.1 us -> 19 us
  starting transfers between devices: 19.9 us -> 12.8 us
    all_to_all x7 -> x8, blocking collectives: 96.6 us -> 114 us  [exchanged(): return lax.all_to_all(x, axis, split_axis=0, concat_axis=0, tiled=True)]
    all_to_all x2 -> x1, waiting for transfers between devices: 11.1 us -> 0.01 us  [exchanged(): return lax.all_to_all(x, axis, split_axis=0, concat_axis=0, tiled=True)]
    all_to_all x2 -> x1, starting transfers between devices: 15.5 us -> 8.47 us  [exchanged(): return lax.all_to_all(x, axis, split_axis=0, concat_axis=0, tiled=True)]
    unnamed x36 -> x34, local copies, waits for them, and re-layouts: 5.13 us -> 4.13 us
  transfers between devices with their start and end apart: 9 -> 8, of which waited for: 4 -> 3; matrix products, arithmetic and copies ran while one was open for 2% -> 2% of each run, Pallas kernels for 3% -> 2%
where the time goes in v2:
time: 163 us; the launch traced here: 162 us
  blocking collectives  114 us (70%)
  waiting for transfers between devices  19 us (12%)
  starting transfers between devices  12.8 us (8%)
  Pallas kernels  10 us (6%)
  local copies, waits for them, and re-layouts  5.38 us (3%)
    all_to_all x8, blocking collectives, exchanged(): return lax.all_to_all(x, axis, split_axis=0, concat_axis=0, tiled=True)  114 us
    ppermute x3, waiting for transfers between devices, layers(): lax.ppermute(later[k], 'y', [(i, (i + k) % ny) for i in range(ny)])  16.9 us
    all_to_all x1, starting transfers between devices, exchanged(): return lax.all_to_all(x, axis, split_axis=0, concat_axis=0, tiled=True)  8.47 us
    unnamed x34, local copies, waits for them, and re-layouts  4.13 us
    ppermute x3, starting transfers between devices, layers(): lax.ppermute(later[k], 'y', [(i, (i + k) % ny) for i in range(ny)])  3.83 us
  transfers between devices with their start and end apart: 8, of which 3 were waited for; matrix products, arithmetic and copies ran while one was open for 2% of the time, Pallas kernels for 2%

profile of v2, /device:TPU:2, one launch (start us, length us, event | category | flops | bytes accessed | tf_op | source)
XLA Modules:
  0.0 161.9 jit_solution(703669578474701771)
XLA Ops:
  0.0 2.4 %pack0.1 = bf16[4,912,128]{2,1,0:T(8,128)(2,1)} custom-call(bf16[2,128,3072]{2,1,0:T(8,128)(2,1)} %gate.3, bf16[2,128,3072]{2,1,0:T(8,128)(2,1)} %value.3, bf16[128,128]{1,0:T(8,128)(2,1)} %bitcast.6, bf16[2,128]{1,0:T(2,128)(2,1)} %gain.1), custom_call_target="tpu_custom_call" | custom-call | flops 1000000 | bytes 933888 | tf_op jit(solution)/shard_map/pack0/pallas_call | solution.py:100
  2.4 18.4 %all_to_all.45.refs_0_ = bf16[4,912,128]{2,1,0:T(8,128)(2,1)S(1)} all-to-all(bf16[4,912,128]{2,1,0:T(8,128)(2,1)} %pack0.1), channel_id=1, replica_groups=mesh['z'=8,'y'=4,'x'=4,'dp'=2] {'y'}, dimensions={0} | all-to-all | bytes 1867776 | tf_op jit(solution)/shard_map/all_to_all | solution.py:25
  20.8 0.0 collective-permute-start
  20.8 0.0 copy-start.13
  20.8 0.3 shard_map.100.refs_2_
  21.1 0.0 copy-start
  21.1 0.0 copy-start.1
  21.2 2.1 %collective-permute-done.refs_1_ = bf16[4,912,128]{2,1,0:T(8,128)(2,1)S(1)} collective-permute-done((bf16[4,912,128]{2,1,0:T(8,128)(2,1)S(1)}, bf16[4,912,128]{2,1,0:T(8,128)(2,1)S(1)}, u32[]{:S(2)}, u32[]{:S(2)}) %collective-permute-start) | collective-permute-done | bytes 933920 | tf_op jit(solution)/shard_map/ppermute | solution.py:519
  23.3 1.2 shard_map.101
  24.5 0.7 copy-done.5
  25.1 8.5 %all-to-all-start.1 = ((bf16[8,200,128]{2,1,0:T(8,128)(2,1)}), bf16[8,200,128]{2,1,0:T(8,128)(2,1)}, u32[]{:S(2)}, u32[]{:S(2)}) async-start(bf16[8,200,128]{2,1,0:T(8,128)(2,1)} %get-tuple-element.23), calls=%async_computation.1 | async-start | bytes 819200 | tf_op jit(solution)/shard_map/all_to_all | solution.py:25
  33.6 0.6 copy.14
  34.2 0.6 copy.16
  34.8 0.6 copy.13
  35.5 0.6 copy.15
  36.1 1.4 copy-done.4
  37.5 2.1 %pack1.1 = (bf16[1536,128]{1,0:T(8,128)(2,1)S(1)}, bf16[1536,128]{1,0:T(8,128)(2,1)S(1)}, bf16[1536,128]{1,0:T(8,128)(2,1)S(1)}, bf16[1536,128]{1,0:T(8,128)(2,1)S(1)}, bf16[1536,128]{1,0:T(8,128)(2,1)S(1)}) custom-call(bf16[2,128,3072]{2,1,0:T(8,128)(2,1)S(1)} %copy-done, bf16[2,128,3072]{2,1,0:T(8,128)(2,1)S(1)} %copy-done.1, ...), custom_call_target="tpu_custom_call" | custom-call | flops 1000000 | bytes 1572864 | tf_op jit(solution)/shard_map/pack1/pallas_call | solution.py:151
  39.6 0.7 copy-done.2
  40.4 0.1 fusion.2
  40.5 0.6 collective-permute-start.1
  41.1 2.1 %collective-permute-start.2 = (bf16[1536,128]{1,0:T(8,128)(2,1)S(1)}, bf16[1536,128]{1,0:T(8,128)(2,1)S(1)}, u32[]{:S(2)}, u32[]{:S(2)}) collective-permute-start(bf16[1536,128]{1,0:T(8,128)(2,1)S(1)} %get-tuple-element.32), channel_id=1, source_target_pairs={{0,16},{8,24},{16,0},{24,8},{1,17},{9,25},{17,1},{25,9},{2,18},{10... | collective-permute-start | bytes 1179656 | tf_op jit(solution)/shard_map/ppermute | solution.py:534
  43.2 1.1 collective-permute-start.3
  44.3 16.8 %collective-permute-done.1.refs_1_.refs_3_ = bf16[1536,128]{1,0:T(8,128)(2,1)S(1)} collective-permute-done((bf16[1536,128]{1,0:T(8,128)(2,1)S(1)}, bf16[1536,128]{1,0:T(8,128)(2,1)S(1)}, u32[]{:S(2)}, u32[]{:S(2)}) %collective-permute-start.1) | collective-permute-done | bytes 393248 | tf_op jit(solution)/shard_map/ppermute | solution.py:534
  61.1 0.0 collective-permute-start.4
  61.1 0.0 collective-permute-done.2.refs_2_.refs_4_
  61.1 0.5 collective-permute-start.5
  61.6 0.1 collective-permute-done.3.refs_3_.refs_5_
  61.7 0.0 collective-permute-start.6
  61.7 0.0 all-to-all-done.1.parts
  61.7 1.3 shard_map.102
  63.0 17.9 %all_to_all.46.hidden = bf16[8,96,128]{2,1,0:T(8,128)(2,1)S(1)} all-to-all(bf16[8,96,128]{2,1,0:T(8,128)(2,1)S(1)} %shard_map.102), channel_id=1, replica_groups=mesh['z'=8,'y'=4,'x'=4,'dp'=2] {'z'}, dimensions={0} | all-to-all | bytes 393216 | tf_op jit(solution)/shard_map/all_to_all | solution.py:25
  80.9 0.3 down00.1.term
  81.2 0.0 collective-permute-done.4.refs_1_.refs_7_.refs_5_
  81.2 0.0 collective-permute-done.5.refs_2_.refs_8_.refs_6_
  81.2 0.0 collective-permute-done.6.refs_3_.refs_9_.refs_7_
  81.2 0.3 down01.1
  81.5 13.3 %all_to_all.47.terms = bf16[16,4,8,128]{3,2,1,0:T(8,128)(2,1)S(1)} all-to-all(bf16[16,4,8,128]{3,2,1,0:T(8,128)(2,1)S(1)} %down01.1), channel_id=1, replica_groups=mesh['z'=8,'y'=4,'x'=4,'dp'=2] {'y','x'}, dimensions={0} | all-to-all | bytes 262144 | tf_op jit(solution)/shard_map/all_to_all | solution.py:25
  94.8 11.1 %all_to_all.48.refs_1_ = bf16[16,4,8,128]{3,2,1,0:T(8,128)(2,1)S(1)} all-to-all(bf16[16,4,8,128]{3,2,1,0:T(8,128)(2,1)S(1)} %add.11), channel_id=1, replica_groups=mesh['z'=8,'y'=4,'x'=4,'dp'=2] {'y','x'}, dimensions={0} | all-to-all | bytes 262144 | tf_op jit(solution)/shard_map/all_to_all | solution.py:25
  105.9 0.5 up1.1
  106.4 15.2 %all_to_all.49.parts = bf16[8,200,128]{2,1,0:T(8,128)(2,1)S(1)} all-to-all(bf16[8,200,128]{2,1,0:T(8,128)(2,1)S(1)} %get-tuple-element.35), channel_id=1, replica_groups=mesh['z'=8,'y'=4,'x'=4,'dp'=2] {'z'}, dimensions={0} | all-to-all | bytes 819200 | tf_op jit(solution)/shard_map/all_to_all | solution.py:25
  121.6 0.3 shard_map.103
  121.9 12.2 %all_to_all.50.hidden = bf16[8,96,128]{2,1,0:T(8,128)(2,1)S(1)} all-to-all(bf16[8,96,128]{2,1,0:T(8,128)(2,1)S(1)} %shard_map.103), channel_id=1, replica_groups=mesh['z'=8,'y'=4,'x'=4,'dp'=2] {'z'}, dimensions={0} | all-to-all | bytes 393216 | tf_op jit(solution)/shard_map/all_to_all | solution.py:25
  134.1 0.3 shard_map.104
  134.4 0.0 copy-start.7
  134.4 13.5 %all_to_all.51.terms = bf16[16,128,128]{2,1,0:T(8,128)(2,1)S(1)} all-to-all(bf16[16,128,128]{2,1,0:T(8,128)(2,1)S(1)} %shard_map.104), channel_id=1, replica_groups=mesh['z'=8,'y'=4,'x'=4,'dp'=2] {'y','x'}, dimensions={0} | all-to-all | bytes 1048576 | tf_op jit(solution)/shard_map/all_to_all | solution.py:25
  147.9 0.2 last.1
  148.1 13.0 %all_to_all.52.parts = bf16[32,8,128]{2,1,0:T(8,128)(2,1)S(1)} all-to-all(bf16[32,8,128]{2,1,0:T(8,128)(2,1)S(1)} %get-tuple-element.38), channel_id=1, replica_groups=mesh['z'=8,'y'=4,'x'=4,'dp'=2] {'z','y'}, dimensions={0} | all-to-all | bytes 131072 | tf_op jit(solution)/shard_map/all_to_all | solution.py:25
  161.1 0.8 norm.1
  (27 shorter events, 0.1 us)
Async XLA Ops:
  20.8 2.5 %collective-permute-start = (bf16[4,912,128]{2,1,0:T(8,128)(2,1)S(1)}, bf16[4,912,128]{2,1,0:T(8,128)(2,1)S(1)}, u32[]{:S(2)}, u32[]{:S(2)}) collective-permute-start(bf16[4,912,128]{2,1,0:T(8,128)(2,1)S(1)} %all_to_all.45.refs_0_), channel_id=1, source_target_pairs={{0,1},{1,0},{2,3},{3,2},{4,5},{5,4},{6,7},{7,6},{8,9},{9,8},{10,11... | collective-permute-start | bytes 2801672 | tf_op jit(solution)/shard_map/ppermute | solution.py:519
  20.8 12.8 %copy-start.14 = (bf16[2,3072]{1,0:T(2,128)(2,1)S(1)}, bf16[2,3072]{1,0:T(2,128)(2,1)}, u32[]{:S(2)}) copy-start(bf16[2,3072]{1,0:T(2,128)(2,1)} %param.16) | copy-start | bytes 36868
  20.8 13.4 %copy-start.15 = (bf16[2,3072]{1,0:T(2,128)(2,1)S(1)}, bf16[2,3072]{1,0:T(2,128)(2,1)}, u32[]{:S(2)}) copy-start(bf16[2,3072]{1,0:T(2,128)(2,1)} %param.17) | copy-start | bytes 36868
  20.8 14.1 %copy-start.12 = (bf16[2,3,3072]{2,0,1:T(2,128)(2,1)S(1)}, bf16[2,3,3072]{2,0,1:T(2,128)(2,1)}, u32[]{:S(2)}) copy-start(bf16[2,3,3072]{2,0,1:T(2,128)(2,1)} %param.14) | copy-start | bytes 110596
  20.8 14.7 %copy-start.13 = (bf16[2,3,3072]{2,0,1:T(2,128)(2,1)S(1)}, bf16[2,3,3072]{2,0,1:T(2,128)(2,1)}, u32[]{:S(2)}) copy-start(bf16[2,3,3072]{2,0,1:T(2,128)(2,1)} %param.15) | copy-start | bytes 110596
  21.1 15.0 %copy-start = (bf16[2,128,3072]{2,1,0:T(8,128)(2,1)S(1)}, bf16[2,128,3072]{2,1,0:T(8,128)(2,1)}, u32[]{:S(2)}) copy-start(bf16[2,128,3072]{2,1,0:T(8,128)(2,1)} %gate.3) | copy-start | bytes 4718596
  21.1 15.0 %copy-start.1 = (bf16[2,128,3072]{2,1,0:T(8,128)(2,1)S(1)}, bf16[2,128,3072]{2,1,0:T(8,128)(2,1)}, u32[]{:S(2)}) copy-start(bf16[2,128,3072]{2,1,0:T(8,128)(2,1)} %value.3) | copy-start | bytes 4718596
  24.5 0.7 copy-start.5
  25.1 36.6 %all-to-all-start.1 = ((bf16[8,200,128]{2,1,0:T(8,128)(2,1)}), bf16[8,200,128]{2,1,0:T(8,128)(2,1)}, u32[]{:S(2)}, u32[]{:S(2)}) async-start(bf16[8,200,128]{2,1,0:T(8,128)(2,1)} %get-tuple-element.23), calls=%async_computation.1 | async-start | bytes 819200 | tf_op jit(solution)/shard_map/all_to_all | solution.py:25
  36.1 1.4 copy-start.4
  37.5 2.8 %copy-start.8 = (bf16[2,3,3072]{2,1,0:T(4,128)(2,1)S(1)}, bf16[2,3,3072]{2,1,0:T(4,128)(2,1)}, u32[]{:S(2)}) copy-start(bf16[2,3,3072]{2,1,0:T(4,128)(2,1)} %copy.13) | copy-start | bytes 110596
  37.5 2.8 %copy-start.9 = (bf16[2,3,3072]{2,1,0:T(4,128)(2,1)S(1)}, bf16[2,3,3072]{2,1,0:T(4,128)(2,1)}, u32[]{:S(2)}) copy-start(bf16[2,3,3072]{2,1,0:T(4,128)(2,1)} %copy.15) | copy-start | bytes 110596
  37.5 2.8 %copy-start.10 = (bf16[2,1,3072]{2,1,0:T(2,128)(2,1)S(1)}, bf16[2,1,3072]{2,1,0:T(2,128)(2,1)}, u32[]{:S(2)}) copy-start(bf16[2,1,3072]{2,1,0:T(2,128)(2,1)} %copy.14) | copy-start | bytes 36868
  37.5 2.8 %copy-start.11 = (bf16[2,1,3072]{2,1,0:T(2,128)(2,1)S(1)}, bf16[2,1,3072]{2,1,0:T(2,128)(2,1)}, u32[]{:S(2)}) copy-start(bf16[2,1,3072]{2,1,0:T(2,128)(2,1)} %copy.16) | copy-start | bytes 36868
  39.6 0.8 copy-start.2
  40.5 40.7 %copy-start.3 = (bf16[1536,128]{1,0:T(8,128)(2,1)S(1)}, bf16[1536,128]{1,0:T(8,128)(2,1)}, u32[]{:S(2)}) copy-start(bf16[1536,128]{1,0:T(8,128)(2,1)} %copy-done.2) | copy-start | bytes 1179652
  40.5 20.6 %collective-permute-start.1 = (bf16[1536,128]{1,0:T(8,128)(2,1)S(1)}, bf16[1536,128]{1,0:T(8,128)(2,1)S(1)}, u32[]{:S(2)}, u32[]{:S(2)}) collective-permute-start(bf16[1536,128]{1,0:T(8,128)(2,1)S(1)} %get-tuple-element.31), channel_id=1, source_target_pairs={{0,8},{8,16},{16,24},{24,0},{1,9},{9,17},{17,25},{25,1},{2,10},{10... | collective-permute-start | bytes 1179656 | tf_op jit(solution)/shard_map/ppermute | solution.py:534
  41.1 20.0 %collective-permute-start.2 = (bf16[1536,128]{1,0:T(8,128)(2,1)S(1)}, bf16[1536,128]{1,0:T(8,128)(2,1)S(1)}, u32[]{:S(2)}, u32[]{:S(2)}) collective-permute-start(bf16[1536,128]{1,0:T(8,128)(2,1)S(1)} %get-tuple-element.32), channel_id=1, source_target_pairs={{0,16},{8,24},{16,0},{24,8},{1,17},{9,25},{17,1},{25,9},{2,18},{10... | collective-permute-start | bytes 1179656 | tf_op jit(solution)/shard_map/ppermute | solution.py:534
  43.2 18.5 %collective-permute-start.3 = (bf16[1536,128]{1,0:T(8,128)(2,1)S(1)}, bf16[1536,128]{1,0:T(8,128)(2,1)S(1)}, u32[]{:S(2)}, u32[]{:S(2)}) collective-permute-start(bf16[1536,128]{1,0:T(8,128)(2,1)S(1)} %get-tuple-element.33), channel_id=1, source_target_pairs={{0,24},{8,0},{16,8},{24,16},{1,25},{9,1},{17,9},{25,17},{2,26},{10... | collective-permute-start | bytes 1179656 | tf_op jit(solution)/shard_map/ppermute | solution.py:534
  61.1 20.1 %collective-permute-start.4 = (bf16[1536,128]{1,0:T(8,128)(2,1)S(1)}, bf16[1536,128]{1,0:T(8,128)(2,1)S(1)}, u32[]{:S(2)}, u32[]{:S(2)}) collective-permute-start(bf16[1536,128]{1,0:T(8,128)(2,1)S(1)} %collective-permute-done.1.refs_1_.refs_3_), channel_id=1, source_target_pairs={{0,1},{1,0},{2,3},{3,2},{4,5},{5,4},{6,7},{7,6},{8,9},{9,8},{10,11... | collective-permute-start | bytes 1179656 | tf_op jit(solution)/shard_map/ppermute | solution.py:538
  61.1 20.1 %collective-permute-start.5 = (bf16[1536,128]{1,0:T(8,128)(2,1)S(1)}, bf16[1536,128]{1,0:T(8,128)(2,1)S(1)}, u32[]{:S(2)}, u32[]{:S(2)}) collective-permute-start(bf16[1536,128]{1,0:T(8,128)(2,1)S(1)} %collective-permute-done.2.refs_2_.refs_4_), channel_id=1, source_target_pairs={{0,1},{1,0},{2,3},{3,2},{4,5},{5,4},{6,7},{7,6},{8,9},{9,8},{10,11... | collective-permute-start | bytes 1179656 | tf_op jit(solution)/shard_map/ppermute | solution.py:538
  61.7 19.5 %collective-permute-start.6 = (bf16[1536,128]{1,0:T(8,128)(2,1)S(1)}, bf16[1536,128]{1,0:T(8,128)(2,1)S(1)}, u32[]{:S(2)}, u32[]{:S(2)}) collective-permute-start(bf16[1536,128]{1,0:T(8,128)(2,1)S(1)} %collective-permute-done.3.refs_3_.refs_5_), channel_id=1, source_target_pairs={{0,1},{1,0},{2,3},{3,2},{4,5},{5,4},{6,7},{7,6},{8,9},{9,8},{10,11... | collective-permute-start | bytes 1179656 | tf_op jit(solution)/shard_map/ppermute | solution.py:538
  81.2 13.6 %copy-start.6 = (bf16[4,144,128]{2,1,0:T(8,128)(2,1)S(1)}, bf16[4,144,128]{2,1,0:T(8,128)(2,1)}, u32[]{:S(2)}) copy-start(bf16[4,144,128]{2,1,0:T(8,128)(2,1)} %copy-done.5) | copy-start | bytes 442372
  134.4 26.7 %copy-start.7 = (bf16[128]{0:T(256)(128)(2,1)S(1)}, bf16[128]{0:T(256)(128)(2,1)}, u32[]{:S(2)}) copy-start(bf16[128]{0:T(256)(128)(2,1)} %param.19) | copy-start | bytes 772

commit v3 on v1

--- a/solution.py
+++ b/solution.py
@@ -351,7 +351,7 @@
             out[:, at] = piece.reshape(ny * nx, -1, LANES).astype(BF16)
         else:
             for i in range(nx):
-                out[at * nx + i] = piece.astype(BF16)
+                out[i * ny + at] = piece.astype(BF16)
 
 
 def lowered(layer, start, half, ny, nx, args):
@@ -370,7 +370,7 @@
 
 def add_kernel(terms, mine, out):
     count, ny, piece, _ = terms.shape
-    place = lax.axis_index("y") * (count // ny) + lax.axis_index("x")
+    place = lax.axis_index("x") * ny + lax.axis_index("y")
     total = terms[0].astype(F32)
     for i in range(1, count):
         total = total + terms[i].astype(F32)
@@ -488,15 +488,15 @@
     hidden = exchanged(hidden, "z")
     far = [later[ny]] + [lax.ppermute(piece, "dp", swap) for piece in near[1:]]
     terms = lowered(0, block, half, ny, nx, [hidden, *near, *far])
-    terms = exchanged(terms, ("y", "x"))
-    fresh = exchanged(added(terms, state), ("y", "x"))
+    terms = exchanged(terms, ("x", "y"))
+    fresh = exchanged(added(terms, state), ("x", "y"))
 
     parts, kept = second_projected(block, ny, nz, [state, fresh, *near, *far])
     hidden = exchanged(gated(1, exchanged(parts, "z"), table, units, length), "z")
     terms = lowered(1, block + half, half, ny, nx, [hidden, *near, *far])
-    terms = exchanged(terms, ("y", "x"))
+    terms = exchanged(terms, ("x", "y"))
     last, squares = finished(terms, kept, nz * ny)
-    squares = exchanged(squares, ("z", "y"))
+    squares = exchanged(squares, ("y", "z"))
     mixed = normed(last, squares, final_gain[None])
     return mixed.reshape(batch_rows, length, width)
 

time: 164 us -> 165 us (level)
  no operation moved by 1% of the time
where the time goes in v3:
time: 165 us; the launch traced here: 163 us
  blocking collectives  96.2 us (58%)
  waiting for transfers between devices  30.1 us (18%)
  starting transfers between devices  19.9 us (12%)
  Pallas kernels  10.5 us (6%)
  local copies, waits for them, and re-layouts  6.4 us (4%)
    all_to_all x7, blocking collectives, exchanged(): return lax.all_to_all(x, axis, split_axis=0, concat_axis=0, tiled=True)  96.2 us
    ppermute x3, waiting for transfers between devices, layers(): lax.ppermute(later[k], 'y', [(i, (i + k) % ny) for i in range(ny)])  16.9 us
    all_to_all x2, starting transfers between devices, exchanged(): return lax.all_to_all(x, axis, split_axis=0, concat_axis=0, tiled=True)  15.5 us
    all_to_all x2, waiting for transfers between devices, exchanged(): return lax.all_to_all(x, axis, split_axis=0, concat_axis=0, tiled=True)  11.1 us
    unnamed x36, local copies, waits for them, and re-layouts  5.13 us
    ppermute x3, starting transfers between devices, layers(): lax.ppermute(later[k], 'y', [(i, (i + k) % ny) for i in range(ny)])  3.83 us
  transfers between devices with their start and end apart: 9, of which 4 were waited for; matrix products, arithmetic and copies ran while one was open for 2% of the time, Pallas kernels for 3%

profile of v3, /device:TPU:2, one launch (start us, length us, event | category | flops | bytes accessed | tf_op | source)
XLA Modules:
  0.0 163.4 jit_solution(2305056651822787139)
XLA Ops:
  0.0 2.4 %pack0.1 = bf16[4,912,128]{2,1,0:T(8,128)(2,1)} custom-call(bf16[2,128,3072]{2,1,0:T(8,128)(2,1)} %gate.3, bf16[2,128,3072]{2,1,0:T(8,128)(2,1)} %value.3, bf16[128,128]{1,0:T(8,128)(2,1)} %bitcast.6, bf16[2,128]{1,0:T(2,128)(2,1)} %gain.1), custom_call_target="tpu_custom_call" | custom-call | flops 1000000 | bytes 933888 | tf_op jit(solution)/shard_map/pack0/pallas_call | solution.py:100
  2.4 18.4 %all_to_all.45.refs_0_ = bf16[4,912,128]{2,1,0:T(8,128)(2,1)S(1)} all-to-all(bf16[4,912,128]{2,1,0:T(8,128)(2,1)} %pack0.1), channel_id=1, replica_groups=mesh['z'=8,'y'=4,'x'=4,'dp'=2] {'y'}, dimensions={0} | all-to-all | bytes 1867776 | tf_op jit(solution)/shard_map/all_to_all | solution.py:25
  20.7 0.0 collective-permute-start
  20.8 0.0 copy-start.14
  20.8 0.3 shard_map.100.refs_2_
  21.1 0.0 copy-start
  21.1 0.0 copy-start.1
  21.1 2.1 %collective-permute-done.refs_1_ = bf16[4,912,128]{2,1,0:T(8,128)(2,1)S(1)} collective-permute-done((bf16[4,912,128]{2,1,0:T(8,128)(2,1)S(1)}, bf16[4,912,128]{2,1,0:T(8,128)(2,1)S(1)}, u32[]{:S(2)}, u32[]{:S(2)}) %collective-permute-start) | collective-permute-done | bytes 933920 | tf_op jit(solution)/shard_map/ppermute | solution.py:470
  23.2 1.2 shard_map.101
  24.5 0.7 copy-done.6
  25.1 8.5 %all-to-all-start.1 = ((bf16[8,200,128]{2,1,0:T(8,128)(2,1)}), bf16[8,200,128]{2,1,0:T(8,128)(2,1)}, u32[]{:S(2)}, u32[]{:S(2)}) async-start(bf16[8,200,128]{2,1,0:T(8,128)(2,1)} %get-tuple-element.23), calls=%async_computation.1 | async-start | bytes 819200 | tf_op jit(solution)/shard_map/all_to_all | solution.py:25
  33.6 0.6 copy.14
  34.2 0.6 copy.16
  34.9 0.6 copy.13
  35.5 0.6 copy.15
  36.1 1.4 copy-done.5
  37.5 2.1 %pack1.1 = (bf16[1536,128]{1,0:T(8,128)(2,1)S(1)}, bf16[1536,128]{1,0:T(8,128)(2,1)S(1)}, bf16[1536,128]{1,0:T(8,128)(2,1)S(1)}, bf16[1536,128]{1,0:T(8,128)(2,1)S(1)}, bf16[1536,128]{1,0:T(8,128)(2,1)S(1)}) custom-call(bf16[2,128,3072]{2,1,0:T(8,128)(2,1)S(1)} %copy-done, bf16[2,128,3072]{2,1,0:T(8,128)(2,1)S(1)} %copy-done.1, ...), custom_call_target="tpu_custom_call" | custom-call | flops 1000000 | bytes 1572864 | tf_op jit(solution)/shard_map/pack1/pallas_call | solution.py:151
  39.6 0.8 copy-done.2
  40.4 0.1 fusion.2
  40.5 0.6 collective-permute-start.1
  41.1 2.1 %collective-permute-start.2 = (bf16[1536,128]{1,0:T(8,128)(2,1)S(1)}, bf16[1536,128]{1,0:T(8,128)(2,1)S(1)}, u32[]{:S(2)}, u32[]{:S(2)}) collective-permute-start(bf16[1536,128]{1,0:T(8,128)(2,1)S(1)} %get-tuple-element.32), channel_id=1, source_target_pairs={{0,16},{8,24},{16,0},{24,8},{1,17},{9,25},{17,1},{25,9},{2,18},{10... | collective-permute-start | bytes 1179656 | tf_op jit(solution)/shard_map/ppermute | solution.py:485
  43.2 1.1 collective-permute-start.3
  44.3 16.7 %collective-permute-done.1.refs_1_.refs_3_ = bf16[1536,128]{1,0:T(8,128)(2,1)S(1)} collective-permute-done((bf16[1536,128]{1,0:T(8,128)(2,1)S(1)}, bf16[1536,128]{1,0:T(8,128)(2,1)S(1)}, u32[]{:S(2)}, u32[]{:S(2)}) %collective-permute-start.1) | collective-permute-done | bytes 393248 | tf_op jit(solution)/shard_map/ppermute | solution.py:485
  61.1 0.0 collective-permute-start.4
  61.1 0.0 collective-permute-done.2.refs_2_.refs_4_
  61.1 0.5 collective-permute-start.5
  61.6 0.1 collective-permute-done.3.refs_3_.refs_5_
  61.7 0.0 collective-permute-start.6
  61.7 0.0 all-to-all-done.1.parts
  61.7 2.1 %shard_map.102 = bf16[8,96,128]{2,1,0:T(8,128)(2,1)} custom-call(bf16[8,200,128]{2,1,0:T(8,128)(2,1)} %all-to-all-done.1.parts, f32[2,8,128]{2,1,0:T(8,128)S(1)} %pad_convert_fusion.table), custom_call_target="tpu_custom_call" | custom-call | flops 1000000 | bytes 409600 | tf_op jit(solution)/shard_map/pallas_call | solution.py:325
  63.8 7.1 %all-to-all-start.2 = ((bf16[8,96,128]{2,1,0:T(8,128)(2,1)}), bf16[8,96,128]{2,1,0:T(8,128)(2,1)S(1)}, u32[]{:S(2)}, u32[]{:S(2)}) async-start(bf16[8,96,128]{2,1,0:T(8,128)(2,1)} %shard_map.102), calls=%async_computation.2 | async-start | bytes 393216 | tf_op jit(solution)/shard_map/all_to_all | solution.py:25
  70.8 0.0 collective-permute-done.4.refs_5_.refs_7_
  70.8 0.0 collective-permute-done.5.refs_6_.refs_8_
  70.9 11.1 %all-to-all-done.2.hidden = bf16[8,96,128]{2,1,0:T(8,128)(2,1)S(1)} async-done(((bf16[8,96,128]{2,1,0:T(8,128)(2,1)}), bf16[8,96,128]{2,1,0:T(8,128)(2,1)S(1)}, u32[]{:S(2)}, u32[]{:S(2)}) %all-to-all-start.2) | async-done | bytes 196640 | tf_op jit(solution)/shard_map/all_to_all | solution.py:25
  82.0 1.0 copy-done.3
  83.0 0.3 shard_map.103
  83.3 13.0 %all_to_all.46.terms = bf16[16,4,8,128]{3,2,1,0:T(8,128)(2,1)S(1)} all-to-all(bf16[16,4,8,128]{3,2,1,0:T(8,128)(2,1)S(1)} %shard_map.103), channel_id=1, replica_groups=mesh['z'=8,'y'=4,'x'=4,'dp'=2] {'x','y'}, dimensions={0} | all-to-all | bytes 262144 | tf_op jit(solution)/shard_map/all_to_all | solution.py:25
  96.4 11.2 %all_to_all.47.refs_1_ = bf16[16,4,8,128]{3,2,1,0:T(8,128)(2,1)S(1)} all-to-all(bf16[16,4,8,128]{3,2,1,0:T(8,128)(2,1)S(1)} %add.11), channel_id=1, replica_groups=mesh['z'=8,'y'=4,'x'=4,'dp'=2] {'x','y'}, dimensions={0} | all-to-all | bytes 262144 | tf_op jit(solution)/shard_map/all_to_all | solution.py:25
  107.6 0.5 up1.1
  108.2 15.2 %all_to_all.48.parts = bf16[8,200,128]{2,1,0:T(8,128)(2,1)S(1)} all-to-all(bf16[8,200,128]{2,1,0:T(8,128)(2,1)S(1)} %get-tuple-element.35), channel_id=1, replica_groups=mesh['z'=8,'y'=4,'x'=4,'dp'=2] {'z'}, dimensions={0} | all-to-all | bytes 819200 | tf_op jit(solution)/shard_map/all_to_all | solution.py:25
  123.3 0.3 shard_map.104
  123.6 12.2 %all_to_all.49.hidden = bf16[8,96,128]{2,1,0:T(8,128)(2,1)S(1)} all-to-all(bf16[8,96,128]{2,1,0:T(8,128)(2,1)S(1)} %shard_map.104), channel_id=1, replica_groups=mesh['z'=8,'y'=4,'x'=4,'dp'=2] {'z'}, dimensions={0} | all-to-all | bytes 393216 | tf_op jit(solution)/shard_map/all_to_all | solution.py:25
  135.8 0.4 shard_map.105
  136.2 0.0 copy-start.8
  136.2 13.0 %all_to_all.50.terms = bf16[16,128,128]{2,1,0:T(8,128)(2,1)S(1)} all-to-all(bf16[16,128,128]{2,1,0:T(8,128)(2,1)S(1)} %shard_map.105), channel_id=1, replica_groups=mesh['z'=8,'y'=4,'x'=4,'dp'=2] {'x','y'}, dimensions={0} | all-to-all | bytes 1048576 | tf_op jit(solution)/shard_map/all_to_all | solution.py:25
  149.2 0.2 last.1
  149.4 13.2 %all_to_all.51.parts = bf16[32,8,128]{2,1,0:T(8,128)(2,1)S(1)} all-to-all(bf16[32,8,128]{2,1,0:T(8,128)(2,1)S(1)} %get-tuple-element.38), channel_id=1, replica_groups=mesh['z'=8,'y'=4,'x'=4,'dp'=2] {'y','z'}, dimensions={0} | all-to-all | bytes 131072 | tf_op jit(solution)/shard_map/all_to_all | solution.py:25
  162.6 0.8 norm.1
  (29 shorter events, 0.1 us)
Async XLA Ops:
  20.7 2.5 %collective-permute-start = (bf16[4,912,128]{2,1,0:T(8,128)(2,1)S(1)}, bf16[4,912,128]{2,1,0:T(8,128)(2,1)S(1)}, u32[]{:S(2)}, u32[]{:S(2)}) collective-permute-start(bf16[4,912,128]{2,1,0:T(8,128)(2,1)S(1)} %all_to_all.45.refs_0_), channel_id=1, source_target_pairs={{0,1},{1,0},{2,3},{3,2},{4,5},{5,4},{6,7},{7,6},{8,9},{9,8},{10,11... | collective-permute-start | bytes 2801672 | tf_op jit(solution)/shard_map/ppermute | solution.py:470
  20.7 12.8 %copy-start.15 = (bf16[2,3072]{1,0:T(2,128)(2,1)S(1)}, bf16[2,3072]{1,0:T(2,128)(2,1)}, u32[]{:S(2)}) copy-start(bf16[2,3072]{1,0:T(2,128)(2,1)} %param.16) | copy-start | bytes 36868
  20.7 13.5 %copy-start.16 = (bf16[2,3072]{1,0:T(2,128)(2,1)S(1)}, bf16[2,3072]{1,0:T(2,128)(2,1)}, u32[]{:S(2)}) copy-start(bf16[2,3072]{1,0:T(2,128)(2,1)} %param.17) | copy-start | bytes 36868
  20.8 14.1 %copy-start.13 = (bf16[2,3,3072]{2,0,1:T(2,128)(2,1)S(1)}, bf16[2,3,3072]{2,0,1:T(2,128)(2,1)}, u32[]{:S(2)}) copy-start(bf16[2,3,3072]{2,0,1:T(2,128)(2,1)} %param.14) | copy-start | bytes 110596
  20.8 14.7 %copy-start.14 = (bf16[2,3,3072]{2,0,1:T(2,128)(2,1)S(1)}, bf16[2,3,3072]{2,0,1:T(2,128)(2,1)}, u32[]{:S(2)}) copy-start(bf16[2,3,3072]{2,0,1:T(2,128)(2,1)} %param.15) | copy-start | bytes 110596
  21.1 15.0 %copy-start = (bf16[2,128,3072]{2,1,0:T(8,128)(2,1)S(1)}, bf16[2,128,3072]{2,1,0:T(8,128)(2,1)}, u32[]{:S(2)}) copy-start(bf16[2,128,3072]{2,1,0:T(8,128)(2,1)} %gate.3) | copy-start | bytes 4718596
  21.1 15.0 %copy-start.1 = (bf16[2,128,3072]{2,1,0:T(8,128)(2,1)S(1)}, bf16[2,128,3072]{2,1,0:T(8,128)(2,1)}, u32[]{:S(2)}) copy-start(bf16[2,128,3072]{2,1,0:T(8,128)(2,1)} %value.3) | copy-start | bytes 4718596
  24.5 0.7 copy-start.6
  25.1 36.6 %all-to-all-start.1 = ((bf16[8,200,128]{2,1,0:T(8,128)(2,1)}), bf16[8,200,128]{2,1,0:T(8,128)(2,1)}, u32[]{:S(2)}, u32[]{:S(2)}) async-start(bf16[8,200,128]{2,1,0:T(8,128)(2,1)} %get-tuple-element.23), calls=%async_computation.1 | async-start | bytes 819200 | tf_op jit(solution)/shard_map/all_to_all | solution.py:25
  36.1 1.4 copy-start.5
  37.5 2.9 %copy-start.9 = (bf16[2,3,3072]{2,1,0:T(4,128)(2,1)S(1)}, bf16[2,3,3072]{2,1,0:T(4,128)(2,1)}, u32[]{:S(2)}) copy-start(bf16[2,3,3072]{2,1,0:T(4,128)(2,1)} %copy.13) | copy-start | bytes 110596
  37.5 2.9 %copy-start.10 = (bf16[2,3,3072]{2,1,0:T(4,128)(2,1)S(1)}, bf16[2,3,3072]{2,1,0:T(4,128)(2,1)}, u32[]{:S(2)}) copy-start(bf16[2,3,3072]{2,1,0:T(4,128)(2,1)} %copy.15) | copy-start | bytes 110596
  37.5 2.9 %copy-start.11 = (bf16[2,1,3072]{2,1,0:T(2,128)(2,1)S(1)}, bf16[2,1,3072]{2,1,0:T(2,128)(2,1)}, u32[]{:S(2)}) copy-start(bf16[2,1,3072]{2,1,0:T(2,128)(2,1)} %copy.14) | copy-start | bytes 36868
  37.5 2.9 %copy-start.12 = (bf16[2,1,3072]{2,1,0:T(2,128)(2,1)S(1)}, bf16[2,1,3072]{2,1,0:T(2,128)(2,1)}, u32[]{:S(2)}) copy-start(bf16[2,1,3072]{2,1,0:T(2,128)(2,1)} %copy.16) | copy-start | bytes 36868
  39.6 0.8 copy-start.2
  40.5 20.6 %collective-permute-start.1 = (bf16[1536,128]{1,0:T(8,128)(2,1)S(1)}, bf16[1536,128]{1,0:T(8,128)(2,1)S(1)}, u32[]{:S(2)}, u32[]{:S(2)}) collective-permute-start(bf16[1536,128]{1,0:T(8,128)(2,1)S(1)} %get-tuple-element.31), channel_id=1, source_target_pairs={{0,8},{8,16},{16,24},{24,0},{1,9},{9,17},{17,25},{25,1},{2,10},{10... | collective-permute-start | bytes 1179656 | tf_op jit(solution)/shard_map/ppermute | solution.py:485
  41.1 20.0 %collective-permute-start.2 = (bf16[1536,128]{1,0:T(8,128)(2,1)S(1)}, bf16[1536,128]{1,0:T(8,128)(2,1)S(1)}, u32[]{:S(2)}, u32[]{:S(2)}) collective-permute-start(bf16[1536,128]{1,0:T(8,128)(2,1)S(1)} %get-tuple-element.32), channel_id=1, source_target_pairs={{0,16},{8,24},{16,0},{24,8},{1,17},{9,25},{17,1},{25,9},{2,18},{10... | collective-permute-start | bytes 1179656 | tf_op jit(solution)/shard_map/ppermute | solution.py:485
  43.2 18.5 %collective-permute-start.3 = (bf16[1536,128]{1,0:T(8,128)(2,1)S(1)}, bf16[1536,128]{1,0:T(8,128)(2,1)S(1)}, u32[]{:S(2)}, u32[]{:S(2)}) collective-permute-start(bf16[1536,128]{1,0:T(8,128)(2,1)S(1)} %get-tuple-element.33), channel_id=1, source_target_pairs={{0,24},{8,0},{16,8},{24,16},{1,25},{9,1},{17,9},{25,17},{2,26},{10... | collective-permute-start | bytes 1179656 | tf_op jit(solution)/shard_map/ppermute | solution.py:485
  61.1 9.8 %collective-permute-start.4 = (bf16[1536,128]{1,0:T(8,128)(2,1)S(1)}, bf16[1536,128]{1,0:T(8,128)(2,1)S(1)}, u32[]{:S(2)}, u32[]{:S(2)}) collective-permute-start(bf16[1536,128]{1,0:T(8,128)(2,1)S(1)} %collective-permute-done.1.refs_1_.refs_3_), channel_id=1, source_target_pairs={{0,1},{1,0},{2,3},{3,2},{4,5},{5,4},{6,7},{7,6},{8,9},{9,8},{10,11... | collective-permute-start | bytes 1179656 | tf_op jit(solution)/shard_map/ppermute | solution.py:489
  61.1 9.8 %collective-permute-start.5 = (bf16[1536,128]{1,0:T(8,128)(2,1)S(1)}, bf16[1536,128]{1,0:T(8,128)(2,1)S(1)}, u32[]{:S(2)}, u32[]{:S(2)}) collective-permute-start(bf16[1536,128]{1,0:T(8,128)(2,1)S(1)} %collective-permute-done.2.refs_2_.refs_4_), channel_id=1, source_target_pairs={{0,1},{1,0},{2,3},{3,2},{4,5},{5,4},{6,7},{7,6},{8,9},{9,8},{10,11... | collective-permute-start | bytes 1179656 | tf_op jit(solution)/shard_map/ppermute | solution.py:489
  61.7 9.1 %collective-permute-start.6 = (bf16[1536,128]{1,0:T(8,128)(2,1)S(1)}, bf16[1536,128]{1,0:T(8,128)(2,1)S(1)}, u32[]{:S(2)}, u32[]{:S(2)}) collective-permute-start(bf16[1536,128]{1,0:T(8,128)(2,1)S(1)} %collective-permute-done.3.refs_3_.refs_5_), channel_id=1, source_target_pairs={{0,1},{1,0},{2,3},{3,2},{4,5},{5,4},{6,7},{7,6},{8,9},{9,8},{10,11... | collective-permute-start | bytes 1179656 | tf_op jit(solution)/shard_map/ppermute | solution.py:489
  61.7 34.6 %copy-start.7 = (bf16[4,144,128]{2,1,0:T(8,128)(2,1)S(1)}, bf16[4,144,128]{2,1,0:T(8,128)(2,1)}, u32[]{:S(2)}) copy-start(bf16[4,144,128]{2,1,0:T(8,128)(2,1)} %copy-done.6) | copy-start | bytes 442372
  63.8 43.9 %copy-start.4 = (bf16[1536,128]{1,0:T(8,128)(2,1)S(1)}, bf16[1536,128]{1,0:T(8,128)(2,1)}, u32[]{:S(2)}) copy-start(bf16[1536,128]{1,0:T(8,128)(2,1)} %copy-done.2) | copy-start | bytes 1179652
  63.8 18.2 %all-to-all-start.2 = ((bf16[8,96,128]{2,1,0:T(8,128)(2,1)}), bf16[8,96,128]{2,1,0:T(8,128)(2,1)S(1)}, u32[]{:S(2)}, u32[]{:S(2)}) async-start(bf16[8,96,128]{2,1,0:T(8,128)(2,1)} %shard_map.102), calls=%async_computation.2 | async-start | bytes 393216 | tf_op jit(solution)/shard_map/all_to_all | solution.py:25
  82.0 1.0 copy-start.3
  136.2 26.4 %copy-start.8 = (bf16[128]{0:T(256)(128)(2,1)S(1)}, bf16[128]{0:T(256)(128)(2,1)}, u32[]{:S(2)}) copy-start(bf16[128]{0:T(256)(128)(2,1)} %param.19) | copy-start | bytes 772
